TPU v7x, 32 devices: a whole 2x2x4 slice. The times are simulated.
32 devices in a mesh: sp: 4 (over y, core), dp: 8 (over z, x).
Axes of the slice: x: 2, y: 2, z: 4, core: 2. Of those that a mesh axis runs over, the one named last changes fastest.
Arguments:
- query_rows: bfloat16 [8, 512, 4, 128], P('dp', 'sp'), may hold values from -6 to 6
- key_rows: bfloat16 [8, 512, 4, 128], P('dp', 'sp'), may hold values from -6 to 6
- value_rows: bfloat16 [8, 512, 4, 128], P('dp', 'sp'), may hold values from -6 to 6
- map_weight: float32 [4], P('sp'), may hold values from 0.3 to 0.8
- head_gain: float32 [128], replicated, may hold values from 0.1 to 1.9
Outputs:
- mixed: bfloat16 [8, 512, 4, 128], P('dp', 'sp')
All inputs are finite; a program needn't handle non-finite values.
Results may differ from a plain program's by a relative error of at most 0.0049.
Values may be sent and summed in bfloat16 or wider, within the bound.
No kernel may reach another device: no remote copies, remote signals or barrier semaphores. Data moves between devices by JAX's collectives and lax.ppermute only.
A program may use at most 64 MiB of HBM per device.

v0:
```python
import math

import jax
import jax.numpy as jnp
from jax import lax
from jax.sharding import PartitionSpec as P

QK = 64
SEGMENT = 64


def map_output(query_map, key_map, value_head):
    length = key_map.shape[0]
    block_len = math.gcd(length, 512)
    key_segment = jnp.arange(length, dtype=jnp.int32) // SEGMENT

    def one_block(start):
        query_block = lax.dynamic_slice_in_dim(query_map, start, block_len, 0)
        query_segment = (start + jnp.arange(block_len, dtype=jnp.int32)) // SEGMENT
        visible = key_segment[None, :] <= query_segment[:, None]
        scores = jnp.dot(query_block, key_map.T, preferred_element_type=jnp.float32) * QK ** (-0.5)
        scores = jnp.where(visible, scores, -jnp.inf)
        scores = scores - jnp.max(scores, axis=-1, keepdims=True)
        raised = jnp.exp(scores)
        weights = raised / jnp.sum(raised, axis=-1, keepdims=True)
        return jnp.dot(weights.astype(jnp.bfloat16), value_head, preferred_element_type=jnp.float32)

    starts = jnp.arange(length // block_len, dtype=jnp.int32) * block_len
    return lax.map(one_block, starts).reshape(length, value_head.shape[1])


def per_heads(query_local, key_local, value_local):
    return lax.map(
        lambda group: map_output(group[0], group[1], group[2]),
        (
            query_local[0].transpose(1, 0, 2),
            key_local[0].transpose(1, 0, 2),
            value_local[0].transpose(1, 0, 2),
        ),
    )


def finish(first_part, second_part, map_weight, head_gain):
    attended = first_part - map_weight[:, None, None] * second_part
    mean_square = jnp.mean(attended * attended, axis=-1, keepdims=True)
    normed = (attended * lax.rsqrt(mean_square + 1e-06) * head_gain).astype(jnp.bfloat16)
    return normed.transpose(1, 0, 2)[None]


def on_device(query_rows, key_rows, value_rows, map_weight, head_gain):
    query_local, key_local, value_local = (
        lax.all_to_all(query_rows, "sp", split_axis=2, concat_axis=1, tiled=True),
        lax.all_to_all(key_rows, "sp", split_axis=2, concat_axis=1, tiled=True),
        lax.all_to_all(value_rows, "sp", split_axis=2, concat_axis=1, tiled=True),
    )
    first_part = per_heads(query_local[..., :QK], key_local[..., :QK], value_local)
    second_part = per_heads(query_local[..., QK:], key_local[..., QK:], value_local)
    normed = finish(first_part, second_part, map_weight, head_gain)
    return lax.all_to_all(normed, "sp", split_axis=1, concat_axis=2, tiled=True)


def solution(mesh):
    return jax.shard_map(
        on_device,
        mesh=mesh,
        in_specs=(
            P("dp", "sp", None, None),
            P("dp", "sp", None, None),
            P("dp", "sp", None, None),
            P("sp"),
            P(),
        ),
        out_specs=P("dp", "sp", None, None),
        check_vma=False,
    )
```

profile of v0, /device:TPU:0, one launch (start us, length us, event | category | flops | bytes accessed | tf_op | source)
XLA Modules:
  0.0 37.9 jit_solution(136135858623358631)
XLA Ops:
  0.0 1.6 %copy.24 = bf16[1,128,4,128]{3,1,0,2:T(8,128)(2,1)} copy(bf16[1,128,4,128]{3,2,1,0:T(4,128)(2,1)} %param.5) | data formatting | bytes 262144 | tf_op args[0]
  1.6 4.4 %all-to-all-start = ((bf16[1,128,4,128]{3,1,0,2:T(8,128)(2,1)}), bf16[1,128,4,128]{3,1,0,2:T(8,128)(2,1)S(1)}, u32[]{:S(2)}, u32[]{:S(2)}) async-start(bf16[1,128,4,128]{3,1,0,2:T(8,128)(2,1)} %copy.24), calls=%async_computation | async-start | bytes 262144 | tf_op jit(solution)/shard_map/all_to_all | solution.py:52
  6.0 0.7 %copy.26 = bf16[1,128,4,128]{3,1,0,2:T(8,128)(2,1)} copy(bf16[1,128,4,128]{3,2,1,0:T(4,128)(2,1)S(1)} %copy-done) | data formatting | bytes 262144 | tf_op args[1]
  6.6 0.3 copy-done.1
  6.9 0.7 %copy.28 = bf16[1,128,4,128]{3,1,0,2:T(8,128)(2,1)} copy(bf16[1,128,4,128]{3,2,1,0:T(4,128)(2,1)S(1)} %copy-done.1) | data formatting | bytes 262144 | tf_op args[2]
  8.3 2.3 %all-to-all-done = bf16[1,128,4,128]{3,1,0,2:T(8,128)(2,1)S(1)} async-done(((bf16[1,128,4,128]{3,1,0,2:T(8,128)(2,1)}), bf16[1,128,4,128]{3,1,0,2:T(8,128)(2,1)S(1)}, u32[]{:S(2)}, u32[]{:S(2)}) %all-to-all-start) | async-done | bytes 131104 | tf_op jit(solution)/shard_map/all_to_all | solution.py:52
  10.6 3.3 %all-to-all-start.1 = ((bf16[1,128,4,128]{3,1,0,2:T(8,128)(2,1)}), bf16[1,128,4,128]{3,1,0,2:T(8,128)(2,1)S(1)}, u32[]{:S(2)}, u32[]{:S(2)}) async-start(bf16[1,128,4,128]{3,1,0,2:T(8,128)(2,1)} %copy.26), calls=%async_computation.1 | async-start | bytes 262144 | tf_op jit(solution)/shard_map/all_to_all | solution.py:53
  13.9 4.6 %all-to-all-done.1 = bf16[1,128,4,128]{3,1,0,2:T(8,128)(2,1)S(1)} async-done(((bf16[1,128,4,128]{3,1,0,2:T(8,128)(2,1)}), bf16[1,128,4,128]{3,1,0,2:T(8,128)(2,1)S(1)}, u32[]{:S(2)}, u32[]{:S(2)}) %all-to-all-start.1) | async-done | bytes 131104 | tf_op jit(solution)/shard_map/all_to_all | solution.py:53
  18.5 3.3 %all-to-all-start.2 = ((bf16[1,128,4,128]{3,1,0,2:T(8,128)(2,1)}), bf16[1,128,4,128]{3,1,0,2:T(8,128)(2,1)S(1)}, u32[]{:S(2)}, u32[]{:S(2)}) async-start(bf16[1,128,4,128]{3,1,0,2:T(8,128)(2,1)} %copy.28), calls=%async_computation.2 | async-start | bytes 262144 | tf_op jit(solution)/shard_map/all_to_all | solution.py:54
  21.8 0.4 %fusion.8 = (f32[512]{0:T(512)S(1)}, f32[512,512]{0,1:T(8,128)S(1)}) fusion(bf16[1,512,1,128]{3,1,2,0:T(8,128)(2,1)S(1)} %bitcast.59, bf16[1,512,1,128]{3,1,2,0:T(8,128)(2,1)S(1)} %bitcast.55, s32[512]{0:T(512)S(1)} %add_select_fusion), kind=kOutput, calls=%fused_computation.27 | convolution fusion | flops 34602496 | bytes 1316864 | tf_op jit(solution)/shard_map/while/body/eval_jaxpr/while/body/eval_jaxpr/dot_general | solution.py:21
  22.2 0.3 fusion.9
  22.5 0.2 fusion.3
  22.7 0.2 fusion.2
  22.9 3.5 %all-to-all-done.2 = bf16[1,128,4,128]{3,1,0,2:T(8,128)(2,1)S(1)} async-done(((bf16[1,128,4,128]{3,1,0,2:T(8,128)(2,1)}), bf16[1,128,4,128]{3,1,0,2:T(8,128)(2,1)S(1)}, u32[]{:S(2)}, u32[]{:S(2)}) %all-to-all-start.2) | async-done | bytes 131104 | tf_op jit(solution)/shard_map/all_to_all | solution.py:54
  26.4 0.3 convolution_multiply_fusion.2
  26.7 0.4 multiply_reduce_fusion
  27.1 0.6 %copy-done.2 = f32[128]{0:T(128)S(1)} copy-done((f32[128]{0:T(128)S(1)}, f32[128]{0:T(128)}, u32[]{:S(2)}) %copy-start.2) | copy-done | bytes 536
  27.8 0.1 fusion.4
  27.8 0.2 copy.31
  28.0 0.5 %broadcast.100 = bf16[]{:T(256)} broadcast(bf16[]{:T(256)} %constant.139), dimensions={} | broadcast | bytes 4
  28.5 1.4 %reduce.2 = bf16[512,128]{1,0:T(8,128)(2,1)S(1)} reduce(bf16[512,1,1,128]{3,2,1,0:T(2,128)(2,1)S(1)} %bitcast.52, bf16[]{:T(256)} %broadcast.100), dimensions={1,2}, to_apply=%bitcast.39.reduce_sub_computation | reduce | bytes 262146
  30.0 7.0 %all_to_all.69 = bf16[4,2,8192]{2,1,0:T(2,128)(2,1)S(1)} all-to-all(bf16[4,2,8192]{2,1,0:T(2,128)(2,1)S(1)} %reshape.64), channel_id=1, replica_groups=mesh['sp'=4,'dp'=8] {'sp'}, dimensions={0} | all-to-all | bytes 262144 | tf_op jit(solution)/shard_map/all_to_all | solution.py:59
  37.0 0.1 reshape.65
  37.1 0.8 %copy.32 = bf16[1,128,4,128]{3,2,1,0:T(4,128)(2,1)} copy(bf16[1,128,4,128]{3,1,2,0:T(8,128)(2,1)S(1)} %bitcast.54) | data formatting | bytes 262144 | tf_op jit(solution)/shard_map/all_to_all | solution.py:59
  (8 shorter events, 0.1 us)
Async XLA Ops:
  1.6 4.4 %copy-start = (bf16[1,128,4,128]{3,2,1,0:T(4,128)(2,1)S(1)}, bf16[1,128,4,128]{3,2,1,0:T(4,128)(2,1)}, u32[]{:S(2)}) copy-start(bf16[1,128,4,128]{3,2,1,0:T(4,128)(2,1)} %param.6) | copy-start | bytes 393220
  1.6 9.0 %all-to-all-start = ((bf16[1,128,4,128]{3,1,0,2:T(8,128)(2,1)}), bf16[1,128,4,128]{3,1,0,2:T(8,128)(2,1)S(1)}, u32[]{:S(2)}, u32[]{:S(2)}) async-start(bf16[1,128,4,128]{3,1,0,2:T(8,128)(2,1)} %copy.24), calls=%async_computation | async-start | bytes 262144 | tf_op jit(solution)/shard_map/all_to_all | solution.py:52
  6.0 1.0 %copy-start.1 = (bf16[1,128,4,128]{3,2,1,0:T(4,128)(2,1)S(1)}, bf16[1,128,4,128]{3,2,1,0:T(4,128)(2,1)}, u32[]{:S(2)}) copy-start(bf16[1,128,4,128]{3,2,1,0:T(4,128)(2,1)} %param.7) | copy-start | bytes 393220
  10.6 7.9 %all-to-all-start.1 = ((bf16[1,128,4,128]{3,1,0,2:T(8,128)(2,1)}), bf16[1,128,4,128]{3,1,0,2:T(8,128)(2,1)S(1)}, u32[]{:S(2)}, u32[]{:S(2)}) async-start(bf16[1,128,4,128]{3,1,0,2:T(8,128)(2,1)} %copy.26), calls=%async_computation.1 | async-start | bytes 262144 | tf_op jit(solution)/shard_map/all_to_all | solution.py:53
  18.5 7.9 %all-to-all-start.2 = ((bf16[1,128,4,128]{3,1,0,2:T(8,128)(2,1)}), bf16[1,128,4,128]{3,1,0,2:T(8,128)(2,1)S(1)}, u32[]{:S(2)}, u32[]{:S(2)}) async-start(bf16[1,128,4,128]{3,1,0,2:T(8,128)(2,1)} %copy.28), calls=%async_computation.2 | async-start | bytes 262144 | tf_op jit(solution)/shard_map/all_to_all | solution.py:54
  27.1 0.7 %copy-start.2 = (f32[128]{0:T(128)S(1)}, f32[128]{0:T(128)}, u32[]{:S(2)}) copy-start(f32[128]{0:T(128)} %param.9) | copy-start | bytes 1540
where the time goes:
time: 38.4 us; the launch traced here: 37.9 us
  starting transfers between devices  11 us (29%)
  waiting for transfers between devices  10.3 us (27%)
  blocking collectives  6.99 us (18%)
  local copies, waits for them, and re-layouts  5.47 us (14%)
  other arithmetic  1.89 us (5%)
  matrix products  1.41 us (4%)
  between operations  0.75 us (2%)
    all_to_all x1, blocking collectives, on_device(): return lax.all_to_all(normed, 'sp', split_axis=1, concat_axis=2, tiled=True)  6.99 us
    all_to_all x1, waiting for transfers between devices, on_device(): lax.all_to_all(key_rows, 'sp', split_axis=2, concat_axis=1, tiled=True)  4.56 us
    unnamed x13, local copies, waits for them, and re-layouts  4.55 us
    all_to_all x1, starting transfers between devices, on_device(): lax.all_to_all(query_rows, 'sp', split_axis=2, concat_axis=1, tiled=True)  4.4 us
    all_to_all x1, waiting for transfers between devices, on_device(): lax.all_to_all(value_rows, 'sp', split_axis=2, concat_axis=1, tiled=True)  3.45 us
    all_to_all x1, starting transfers between devices, on_device(): lax.all_to_all(value_rows, 'sp', split_axis=2, concat_axis=1, tiled=True)  3.33 us
    all_to_all x1, starting transfers between devices, on_device(): lax.all_to_all(key_rows, 'sp', split_axis=2, concat_axis=1, tiled=True)  3.32 us
    all_to_all x1, waiting for transfers between devices, on_device(): lax.all_to_all(query_rows, 'sp', split_axis=2, concat_axis=1, tiled=True)  2.32 us
  transfers between devices with their start and end apart: 3, of which 3 were waited for; matrix products, arithmetic and copies ran while one was open for 6% of the time, Pallas kernels for 0%

commit v1 on v0

v1 whole, which is shorter than its diff:
```python
import functools
import math

import jax
import jax.numpy as jnp
from jax import lax
from jax.experimental import pallas as pl
from jax.experimental.pallas import tpu as pltpu
from jax.sharding import PartitionSpec as P

QK = 64
SEGMENT = 64
CORES = 2
EXP_SCALE = math.log2(math.e) * QK ** (-0.5)
SPARE_BYTES = 8 << 20
NT = (((1,), (1,)), ((), ()))


def each_head(heads, body):
    if heads <= 8:
        for head in range(heads):
            body(head)
    else:
        lax.fori_loop(0, heads, lambda head, c: (body(head), c)[1], 0)


def sources(peers):
    here = lax.axis_index("sp")
    cores = CORES if peers % CORES == 0 else 1
    chips = peers // cores
    chip, core = here // cores, here % cores
    straight = [lax.rem(chip + chips - r, chips) * cores + core for r in range(chips)]
    crossed = [lax.rem(chip + chips - r, chips) * cores + cores - 1 - core for r in range(chips)]
    if cores == 1:
        return here, [here], straight[1:], []
    return here, [here, crossed[0]], straight[1:], crossed[1:]


def head_rows(ref, head, heads, tokens):
    return ref[pl.ds(head, tokens, stride=heads), :].astype(jnp.bfloat16)


def hide(scores, here, source, tokens):
    queries = here * tokens + lax.rem(lax.broadcasted_iota(jnp.int32, scores.shape, 0), tokens)
    keys = source * tokens + lax.broadcasted_iota(jnp.int32, scores.shape, 1)
    return jnp.where(keys // SEGMENT <= queries // SEGMENT, scores, -jnp.inf)


def weigh(stacked, key_refs, srcs, here, head, heads, tokens, floor):
    scores = []
    for ref, source in zip(key_refs, srcs):
        block = lax.dot_general(stacked, head_rows(ref, head, heads, tokens), NT, preferred_element_type=jnp.float32)
        scores.append(hide(block, here, source, tokens))
    top = functools.reduce(jnp.maximum, scores)
    top = jnp.max(top, axis=1, keepdims=True)
    top = jnp.broadcast_to(top, scores[0].shape)
    if floor is not None:
        top = jnp.maximum(top, floor)
    raised = [jnp.exp2((block - top) * EXP_SCALE) for block in scores]
    total = jnp.sum(functools.reduce(jnp.add, raised), axis=1, keepdims=True)
    return top, raised, jnp.broadcast_to(total, scores[0].shape)


def widen(refs, wide):
    for i, ref in enumerate(refs):
        wide[i] = ref[...].astype(jnp.float32)
    return [wide.at[i] for i in range(len(refs))]


def near_scores(peers, heads, tokens, query, *refs):
    keys, (stacked, raised, top, total, wide) = refs[:-5], refs[-5:]
    here, near, _, _ = sources(peers)
    query_wide, *keys_wide = widen((query, *keys), wide)

    def body(head):
        rows = head_rows(query_wide, head, heads, tokens)
        first = lax.broadcasted_iota(jnp.int32, rows.shape, 1) < QK
        zero = jnp.zeros_like(rows)
        both = jnp.concatenate([jnp.where(first, rows, zero), jnp.where(first, zero, rows)], axis=0)
        stacked[head] = both
        peak, blocks, mass = weigh(both, keys_wide, near, here, head, heads, tokens, None)
        top[head] = peak
        total[head] = mass
        for i, block in enumerate(blocks):
            raised[i, head] = block

    each_head(heads, body)


def straight_scores(peers, heads, tokens, stacked, floor, *refs):
    keys, (raised, top, total, wide) = refs[:-4], refs[-4:]
    here, _, straight, _ = sources(peers)
    keys_wide = widen(keys, wide)

    def body(head):
        peak, blocks, mass = weigh(stacked[head], keys_wide, straight, here, head, heads, tokens, floor[head])
        top[head] = peak
        total[head] = mass
        for i, block in enumerate(blocks):
            raised[i, head] = block

    each_head(heads, body)


def last_scores(peers, heads, tokens, counts, *refs):
    refs = list(refs)
    stacked, near_raised, near_top, near_total, far_raised, far_top, far_total = refs[:7]
    n_near, n_straight, n_crossed = counts
    at = 7
    map_weights, at = refs[at : at + n_near + n_straight + n_crossed], at + n_near + n_straight + n_crossed
    values, at = refs[at : at + n_near + n_straight], at + n_near + n_straight
    keys, at = refs[at : at + n_crossed], at + n_crossed
    weights, partial, wide, values_wide = refs[at:]
    here, near, straight, crossed = sources(peers)
    keys_wide = widen(keys, wide)
    value_refs = widen(values, values_wide)
    per_peer = heads // peers

    def body(head):
        second = jnp.zeros((1, 1), jnp.float32)
        for ref, source in zip(map_weights, near + straight + crossed):
            for own in range(per_peer):
                second += jnp.where(source * per_peer + own == head, ref[:, own : own + 1], 0.0)
        peak, blocks, mass = weigh(stacked[head], keys_wide, crossed, here, head, heads, tokens, far_top[head])
        near_scale = jnp.exp2((near_top[head] - peak) * EXP_SCALE)
        far_scale = jnp.exp2((far_top[head] - peak) * EXP_SCALE)
        inverse = 1.0 / (near_scale * near_total[head] + far_scale * far_total[head] + mass)
        inverse = jnp.concatenate([inverse[:tokens], -second * inverse[tokens:]], axis=0)
        near_scale = near_scale * inverse
        far_scale = far_scale * inverse

        def joined(block, scale):
            scaled = block * scale
            return (scaled[:tokens] + scaled[tokens:]).astype(jnp.bfloat16)

        for i, block in enumerate(blocks):
            weights[i, head] = joined(block, inverse)
        ready = [joined(near_raised[i, head], near_scale) for i in range(n_near)]
        ready += [joined(far_raised[i, head], far_scale) for i in range(n_straight)]
        acc = None
        for weight, ref in zip(ready, value_refs):
            part = jnp.dot(weight, head_rows(ref, head, heads, tokens), preferred_element_type=jnp.float32)
            acc = part if acc is None else acc + part
        partial[head] = acc

    each_head(heads, body)


def finish(heads, tokens, weights, partial, gain, *refs):
    values, (out, wide, out_wide) = refs[:-3], refs[-3:]
    value_refs = widen(values, wide)

    def body(head):
        attended = partial[head]
        for i, ref in enumerate(value_refs):
            attended += jnp.dot(weights[i, head], head_rows(ref, head, heads, tokens), preferred_element_type=jnp.float32)
        mean_square = jnp.mean(attended * attended, axis=1, keepdims=True)
        out_wide[pl.ds(head, tokens, stride=heads), :] = attended * lax.rsqrt(mean_square + 1e-06) * gain[...]

    each_head(heads, body)
    out[...] = out_wide[...].astype(out.dtype)


def kernel(body, outs, scratch, vmem_out=True):
    space = pl.BlockSpec(memory_space=pltpu.VMEM)
    limit = SPARE_BYTES + sum(4 * math.prod(s.shape) for s in scratch)

    def call(*args):
        args = [pltpu.with_memory_space_constraint(a, pltpu.VMEM) if a.size > 1024 else a for a in args]
        return pl.pallas_call(
            body,
            out_shape=outs,
            in_specs=[space] * len(args),
            out_specs=jax.tree.map(lambda _: space, outs),
            scratch_shapes=scratch,
            compiler_params=pltpu.CompilerParams(vmem_limit_bytes=limit),
        )(*args)

    return call


def on_device(query_rows, key_rows, value_rows, map_weight, head_gain):
    peers = lax.axis_size("sp")
    _, tokens, heads, width = query_rows.shape
    cores = CORES if peers % CORES == 0 else 1
    chips = peers // cores
    rows = tokens * heads

    def turn(x, by):
        return lax.ppermute(x, "sp", [(i, (i + by * cores) % peers) for i in range(peers)])

    def swap(x):
        return lax.ppermute(x, "sp", [(i, i // cores * cores + cores - 1 - i % cores) for i in range(peers)])

    def flat(x):
        return x.reshape(rows, width)

    shift = range(1, chips)
    key_far = [turn(key_rows, r) for r in shift]
    value_far = [turn(value_rows, r) for r in shift]
    weight_far = [turn(map_weight, r) for r in shift]
    crossing = cores > 1
    key_near = [key_rows] + ([swap(key_rows)] if crossing else [])
    value_near = [value_rows] + ([swap(value_rows)] if crossing else [])
    weight_near = [map_weight] + ([swap(map_weight)] if crossing else [])
    key_last = [swap(x) for x in key_far] if crossing else []
    value_last = [swap(x) for x in value_far] if crossing else []
    weight_last = [swap(x) for x in weight_far] if crossing else []
    n_near, n_far, n_last = len(key_near), len(key_far), len(key_last)

    f32 = lambda *s: jax.ShapeDtypeStruct(s, jnp.float32)
    bf16 = lambda *s: jax.ShapeDtypeStruct(s, jnp.bfloat16)
    wide = lambda n: pltpu.VMEM((n, rows, width), jnp.float32)
    stat = f32(heads, 2 * tokens, tokens)
    blocks = lambda n: f32(n, heads, 2 * tokens, tokens)

    stacked, near_raised, near_top, near_total = kernel(
        functools.partial(near_scores, peers, heads, tokens),
        (bf16(heads, 2 * tokens, width), blocks(n_near), stat, stat),
        [wide(1 + n_near)],
    )(flat(query_rows), *map(flat, key_near))
    far_raised, far_top, far_total = kernel(
        functools.partial(straight_scores, peers, heads, tokens),
        (blocks(n_far), stat, stat),
        [wide(n_far)],
    )(stacked, near_top, *map(flat, key_far))
    weights, partial = kernel(
        functools.partial(last_scores, peers, heads, tokens, (n_near, n_far, n_last)),
        (bf16(n_last, heads, tokens, tokens), f32(heads, tokens, width)),
        [wide(n_last), wide(n_near + n_far)],
    )(
        stacked, near_raised, near_top, near_total, far_raised, far_top, far_total,
        *(w.reshape(1, -1) for w in weight_near + weight_far + weight_last),
        *map(flat, value_near + value_far),
        *map(flat, key_last),
    )
    mixed = kernel(
        functools.partial(finish, heads, tokens),
        bf16(rows, width),
        [wide(n_last), pltpu.VMEM((rows, width), jnp.float32)],
    )(weights, partial, head_gain.reshape(1, -1), *map(flat, value_last))
    return mixed.reshape(query_rows.shape)


def solution(mesh):
    rows = P("dp", "sp", None, None)
    return jax.shard_map(
        on_device,
        mesh=mesh,
        in_specs=(rows, rows, rows, P("sp"), P()),
        out_specs=rows,
        check_vma=False,
    )
```

time: 38.4 us -> 22.2 us (0.58)
  blocking collectives: 6.99 us -> 0 us
  Pallas kernels: 0 us -> 5.27 us
  starting transfers between devices: 11 us -> 5.79 us
  waiting for transfers between devices: 10.3 us -> 7.37 us
  local copies, waits for them, and re-layouts: 5.47 us -> 2.78 us
  other arithmetic: 1.89 us -> 0 us
  matrix products: 1.41 us -> 0 us
    all_to_all x3 -> x0, starting transfers between devices: 11 us -> none  [the longest x1 4.4 us: on_device(): lax.all_to_all(query_rows, 'sp', split_axis=2, concat_axis=1, tiled=True)]
    all_to_all x3 -> x0, waiting for transfers between devices: 10.3 us -> none  [the longest x1 4.56 us: on_device(): lax.all_to_all(key_rows, 'sp', split_axis=2, concat_axis=1, tiled=True)]
    ppermute x0 -> x9, waiting for transfers between devices: none -> 7.37 us  [the longest x3 7.35 us: turn(): lax.ppermute(x, 'sp', [(i, (i + by * cores) % peers) for i in range(peers)])]
    all_to_all x1 -> x0, blocking collectives: 6.99 us -> none  [on_device(): return lax.all_to_all(normed, 'sp', split_axis=1, concat_axis=2, tiled=True)]
    ppermute x0 -> x9, starting transfers between devices: none -> 5.79 us  [the longest x3 4.76 us: turn(): lax.ppermute(x, 'sp', [(i, (i + by * cores) % peers) for i in range(peers)])]
    pallas_call x0 -> x4, Pallas kernels: none -> 5.27 us  [call(): pl.pallas_call(body, out_shape=outs, in_specs=[space] * len(args), out_sp...]
    unnamed x13 -> x8, local copies, waits for them, and re-layouts: 4.55 us -> 2.78 us
    dot_general x4 -> x0, matrix products: 1.41 us -> none  [the longest x2 0.71 us: one_block(): jnp.dot(query_block, key_map.T, preferred_element_type=jnp.float32)]
  transfers between devices with their start and end apart: 3 -> 9, of which waited for: 3 -> 3; matrix products, arithmetic and copies ran while one was open for 6% -> 0% of each run, Pallas kernels for 0% -> 20%
where the time goes in v1:
time: 22.2 us; the launch traced here: 22 us
  waiting for transfers between devices  7.37 us (33%)
  starting transfers between devices  5.79 us (26%)
  Pallas kernels  5.27 us (24%)
  local copies, waits for them, and re-layouts  2.78 us (13%)
  between operations  0.77 us (3%)
    ppermute x3, waiting for transfers between devices, turn(): lax.ppermute(x, 'sp', [(i, (i + by * cores) % peers) for i in range(peers)])  7.35 us
    pallas_call x4, Pallas kernels, call(): pl.pallas_call(body, out_shape=outs, in_specs=[space] * len(args), out_sp...  5.27 us
    ppermute x3, starting transfers between devices, turn(): lax.ppermute(x, 'sp', [(i, (i + by * cores) % peers) for i in range(peers)])  4.76 us
    unnamed x8, local copies, waits for them, and re-layouts  2.78 us
    ppermute x6, starting transfers between devices, swap(): lax.ppermute(x, 'sp', [(i, i // cores * cores + cores - 1 - i % cores) fo...  1.03 us
  transfers between devices with their start and end apart: 9, of which 3 were waited for; matrix products, arithmetic and copies ran while one was open for 0% of the time, Pallas kernels for 20%

profile of v1, /device:TPU:0, one launch (start us, length us, event | category | flops | bytes accessed | tf_op | source)
XLA Modules:
  0.0 22.0 jit_solution(5633880046286012640)
XLA Ops:
  0.0 3.0 %collective-permute-start.1 = (bf16[1,128,4,128]{3,2,1,0:T(4,128)(2,1)}, bf16[1,128,4,128]{3,2,1,0:T(4,128)(2,1)S(1)}, u32[]{:S(2)}, u32[]{:S(2)}) collective-permute-start(bf16[1,128,4,128]{3,2,1,0:T(4,128)(2,1)} %param.6), channel_id=1, source_target_pairs={{0,16},{8,24},{16,0},{24,8},{1,17},{9,25},{17,1},{25,9},{2,18},{10... | collective-permute-start | bytes 393224 | tf_op jit(solution)/shard_map/ppermute | solution.py:190
  3.0 0.0 collective-permute-start.6
  3.0 0.0 collective-permute-start
  3.0 0.5 %collective-permute-start.5 = (bf16[1,128,4,128]{3,2,1,0:T(4,128)(2,1)}, bf16[1,128,4,128]{3,2,1,0:T(4,128)(2,1)S(1)}, u32[]{:S(2)}, u32[]{:S(2)}) collective-permute-start(bf16[1,128,4,128]{3,2,1,0:T(4,128)(2,1)} %param.7), channel_id=1, source_target_pairs={{0,8},{8,0},{16,24},{24,16},{1,9},{9,1},{17,25},{25,17},{2,10},{10... | collective-permute-start | bytes 393224 | tf_op jit(solution)/shard_map/ppermute | solution.py:193
  3.5 4.0 %collective-permute-done.1 = bf16[1,128,4,128]{3,2,1,0:T(4,128)(2,1)S(1)} collective-permute-done((bf16[1,128,4,128]{3,2,1,0:T(4,128)(2,1)}, bf16[1,128,4,128]{3,2,1,0:T(4,128)(2,1)S(1)}, u32[]{:S(2)}, u32[]{:S(2)}) %collective-permute-start.1) | collective-permute-done | bytes 131104 | tf_op jit(solution)/shard_map/ppermute | solution.py:190
  7.6 0.0 collective-permute-start.7
  7.6 2.0 %collective-permute-done.6 = bf16[1,128,4,128]{3,2,1,0:T(4,128)(2,1)S(1)} collective-permute-done((bf16[1,128,4,128]{3,2,1,0:T(4,128)(2,1)}, bf16[1,128,4,128]{3,2,1,0:T(4,128)(2,1)S(1)}, u32[]{:S(2)}, u32[]{:S(2)}) %collective-permute-start.6) | collective-permute-done | bytes 131104 | tf_op jit(solution)/shard_map/ppermute | solution.py:190
  9.5 1.7 %collective-permute-start.3 = (f32[1]{0:T(128)}, f32[1]{0:T(128)}, u32[]{:S(2)}, u32[]{:S(2)}) collective-permute-start(f32[1]{0:T(128)} %param.8), channel_id=1, source_target_pairs={{0,16},{8,24},{16,0},{24,8},{1,17},{9,25},{17,1},{25,9},{2,18},{10... | collective-permute-start | bytes 20 | tf_op jit(solution)/shard_map/ppermute | solution.py:190
  11.9 1.4 %collective-permute-done.3 = f32[1]{0:T(128)} collective-permute-done((f32[1]{0:T(128)}, f32[1]{0:T(128)}, u32[]{:S(2)}, u32[]{:S(2)}) %collective-permute-start.3) | collective-permute-done | bytes 36 | tf_op jit(solution)/shard_map/ppermute | solution.py:190
  13.3 0.0 collective-permute-start.2
  13.3 0.0 collective-permute-done
  13.3 0.5 %collective-permute-start.4 = (f32[1]{0:T(128)}, f32[1]{0:T(128)}, u32[]{:S(2)}, u32[]{:S(2)}) collective-permute-start(f32[1]{0:T(128)} %collective-permute-done.3), channel_id=1, source_target_pairs={{0,8},{8,0},{16,24},{24,16},{1,9},{9,1},{17,25},{25,17},{2,10},{10... | collective-permute-start | bytes 20 | tf_op jit(solution)/shard_map/ppermute | solution.py:193
  13.8 0.9 %copy-done = bf16[1,128,4,128]{3,2,1,0:T(4,128)(2,1)S(1)} copy-done((bf16[1,128,4,128]{3,2,1,0:T(4,128)(2,1)S(1)}, bf16[1,128,4,128]{3,2,1,0:T(4,128)(2,1)}, u32[]{:S(2)}) %copy-start) | copy-done | bytes 131096
  14.7 0.9 %copy-done.1 = bf16[1,128,4,128]{3,2,1,0:T(4,128)(2,1)S(1)} copy-done((bf16[1,128,4,128]{3,2,1,0:T(4,128)(2,1)S(1)}, bf16[1,128,4,128]{3,2,1,0:T(4,128)(2,1)}, u32[]{:S(2)}) %copy-start.1) | copy-done | bytes 131096
  15.6 0.6 %shard_map.55 = (bf16[4,256,128]{2,1,0:T(8,128)(2,1)S(1)}, f32[2,4,256,128]{3,2,1,0:T(8,128)S(1)}, f32[4,256,128]{2,1,0:T(8,128)S(1)}, f32[4,256,128]{2,1,0:T(8,128)S(1)}) custom-call(bf16[512,128]{1,0:T(8,128)(2,1)S(1)} %bitcast.16, bf16[512,128]{1,0:T(8,128)(2,1)S(1)} %bitcast.17, bf16[512,128]{1,0:T(8,128)(2,1)S(1)} %bitcast.23), custom_call_target="tpu_custom_call" | custom-call | tf_op jit(solution)/shard_map/pallas_call | solution.py:170
  16.3 0.0 copy-start.2
  16.3 0.5 %shard_map.56 = (f32[1,4,256,128]{3,2,1,0:T(8,128)S(1)}, f32[4,256,128]{2,1,0:T(8,128)S(1)}, f32[4,256,128]{2,1,0:T(8,128)S(1)}) custom-call(bf16[4,256,128]{2,1,0:T(8,128)(2,1)S(1)} %get-tuple-element.14.stacked.refs_0_, f32[4,256,128]{2,1,0:T(8,128)S(1)} %get-tuple-element.16.floor.refs_2_, bf16[512,128]{1,0:T(8,128)(2,1)S(1)} %bitcast.20), custom_call_target="tpu_custom_call" | custom-call | tf_op jit(solution)/shard_map/pallas_call | solution.py:170
  16.9 0.0 collective-permute-done.5
  16.9 0.3 %copy-done.2 = bf16[1,128,4,128]{3,2,1,0:T(4,128)(2,1)S(1)} copy-done((bf16[1,128,4,128]{3,2,1,0:T(4,128)(2,1)S(1)}, bf16[1,128,4,128]{3,2,1,0:T(4,128)(2,1)}, u32[]{:S(2)}) %copy-start.2) | copy-done | bytes 131096
  17.2 3.1 %shard_map.57 = (bf16[1,4,128,128]{3,2,1,0:T(8,128)(2,1)S(1)}, f32[4,128,128]{2,1,0:T(8,128)S(1)}) custom-call(bf16[4,256,128]{2,1,0:T(8,128)(2,1)S(1)} %get-tuple-element.14.stacked.refs_0_, f32[2,4,256,128]{3,2,1,0:T(8,128)S(1)} %get-tuple-element.15.refs_1_, f32[4,256,128]{2,1,0:T(8,128)S(1)} %get-tuple-element.16.floor.refs_2_, ...), custom_call_target="tpu_custom_call" | custom-call | tf_op jit(solution)/shard_map/pallas_call | solution.py:170
  20.3 0.0 collective-permute-done.8
  20.3 0.0 copy-start.3
  20.3 0.6 %copy-done.3 = f32[128]{0:T(128)S(1)} copy-done((f32[128]{0:T(128)S(1)}, f32[128]{0:T(128)}, u32[]{:S(2)}) %copy-start.3) | copy-done | bytes 536
  21.0 1.0 %shard_map.58 = bf16[512,128]{1,0:T(8,128)(2,1)} custom-call(bf16[1,4,128,128]{3,2,1,0:T(8,128)(2,1)S(1)} %get-tuple-element.21.weights, f32[4,128,128]{2,1,0:T(8,128)S(1)} %get-tuple-element.22.partial, f32[1,128]{1,0:T(1,128)S(1)} %bitcast.25, bf16[512,128]{1,0:T(8,128)(2,1)S(1)} %bitcast.24), custom_call_target="tpu_custom_call" | custom-call | tf_op jit(solution)/shard_map/pallas_call | solution.py:170
  (6 shorter events, 0.0 us)
Async XLA Ops:
  0.0 7.5 %collective-permute-start.1 = (bf16[1,128,4,128]{3,2,1,0:T(4,128)(2,1)}, bf16[1,128,4,128]{3,2,1,0:T(4,128)(2,1)S(1)}, u32[]{:S(2)}, u32[]{:S(2)}) collective-permute-start(bf16[1,128,4,128]{3,2,1,0:T(4,128)(2,1)} %param.6), channel_id=1, source_target_pairs={{0,16},{8,24},{16,0},{24,8},{1,17},{9,25},{17,1},{25,9},{2,18},{10... | collective-permute-start | bytes 393224 | tf_op jit(solution)/shard_map/ppermute | solution.py:190
  3.0 6.5 %collective-permute-start.6 = (bf16[1,128,4,128]{3,2,1,0:T(4,128)(2,1)}, bf16[1,128,4,128]{3,2,1,0:T(4,128)(2,1)S(1)}, u32[]{:S(2)}, u32[]{:S(2)}) collective-permute-start(bf16[1,128,4,128]{3,2,1,0:T(4,128)(2,1)} %param.7), channel_id=1, source_target_pairs={{0,16},{8,24},{16,0},{24,8},{1,17},{9,25},{17,1},{25,9},{2,18},{10... | collective-permute-start | bytes 393224 | tf_op jit(solution)/shard_map/ppermute | solution.py:190
  3.0 10.3 %collective-permute-start = (bf16[1,128,4,128]{3,2,1,0:T(4,128)(2,1)}, bf16[1,128,4,128]{3,2,1,0:T(4,128)(2,1)S(1)}, u32[]{:S(2)}, u32[]{:S(2)}) collective-permute-start(bf16[1,128,4,128]{3,2,1,0:T(4,128)(2,1)} %param.6), channel_id=1, source_target_pairs={{0,8},{8,0},{16,24},{24,16},{1,9},{9,1},{17,25},{25,17},{2,10},{10... | collective-permute-start | bytes 393224 | tf_op jit(solution)/shard_map/ppermute | solution.py:193
  3.0 13.8 %collective-permute-start.5 = (bf16[1,128,4,128]{3,2,1,0:T(4,128)(2,1)}, bf16[1,128,4,128]{3,2,1,0:T(4,128)(2,1)S(1)}, u32[]{:S(2)}, u32[]{:S(2)}) collective-permute-start(bf16[1,128,4,128]{3,2,1,0:T(4,128)(2,1)} %param.7), channel_id=1, source_target_pairs={{0,8},{8,0},{16,24},{24,16},{1,9},{9,1},{17,25},{25,17},{2,10},{10... | collective-permute-start | bytes 393224 | tf_op jit(solution)/shard_map/ppermute | solution.py:193
  7.6 9.3 %collective-permute-start.7 = (bf16[1,128,4,128]{3,2,1,0:T(4,128)(2,1)S(1)}, bf16[1,128,4,128]{3,2,1,0:T(4,128)(2,1)S(1)}, u32[]{:S(2)}, u32[]{:S(2)}) collective-permute-start(bf16[1,128,4,128]{3,2,1,0:T(4,128)(2,1)S(1)} %collective-permute-done.1), channel_id=1, source_target_pairs={{0,8},{8,0},{16,24},{24,16},{1,9},{9,1},{17,25},{25,17},{2,10},{10... | collective-permute-start | bytes 393224 | tf_op jit(solution)/shard_map/ppermute | solution.py:193
  9.5 10.8 %collective-permute-start.8 = (bf16[1,128,4,128]{3,2,1,0:T(4,128)(2,1)S(1)}, bf16[1,128,4,128]{3,2,1,0:T(4,128)(2,1)S(1)}, u32[]{:S(2)}, u32[]{:S(2)}) collective-permute-start(bf16[1,128,4,128]{3,2,1,0:T(4,128)(2,1)S(1)} %collective-permute-done.6), channel_id=1, source_target_pairs={{0,8},{8,0},{16,24},{24,16},{1,9},{9,1},{17,25},{25,17},{2,10},{10... | collective-permute-start | bytes 393224 | tf_op jit(solution)/shard_map/ppermute | solution.py:193
  9.5 3.8 %collective-permute-start.3 = (f32[1]{0:T(128)}, f32[1]{0:T(128)}, u32[]{:S(2)}, u32[]{:S(2)}) collective-permute-start(f32[1]{0:T(128)} %param.8), channel_id=1, source_target_pairs={{0,16},{8,24},{16,0},{24,8},{1,17},{9,25},{17,1},{25,9},{2,18},{10... | collective-permute-start | bytes 20 | tf_op jit(solution)/shard_map/ppermute | solution.py:190
  13.3 3.5 %collective-permute-start.2 = (f32[1]{0:T(128)}, f32[1]{0:T(128)}, u32[]{:S(2)}, u32[]{:S(2)}) collective-permute-start(f32[1]{0:T(128)} %param.8), channel_id=1, source_target_pairs={{0,8},{8,0},{16,24},{24,16},{1,9},{9,1},{17,25},{25,17},{2,10},{10... | collective-permute-start | bytes 20 | tf_op jit(solution)/shard_map/ppermute | solution.py:193
  13.3 3.5 %collective-permute-start.4 = (f32[1]{0:T(128)}, f32[1]{0:T(128)}, u32[]{:S(2)}, u32[]{:S(2)}) collective-permute-start(f32[1]{0:T(128)} %collective-permute-done.3), channel_id=1, source_target_pairs={{0,8},{8,0},{16,24},{24,16},{1,9},{9,1},{17,25},{25,17},{2,10},{10... | collective-permute-start | bytes 20 | tf_op jit(solution)/shard_map/ppermute | solution.py:193
  13.8 0.9 %copy-start = (bf16[1,128,4,128]{3,2,1,0:T(4,128)(2,1)S(1)}, bf16[1,128,4,128]{3,2,1,0:T(4,128)(2,1)}, u32[]{:S(2)}) copy-start(bf16[1,128,4,128]{3,2,1,0:T(4,128)(2,1)} %param.5) | copy-start | bytes 393220
  14.7 0.9 %copy-start.1 = (bf16[1,128,4,128]{3,2,1,0:T(4,128)(2,1)S(1)}, bf16[1,128,4,128]{3,2,1,0:T(4,128)(2,1)}, u32[]{:S(2)}) copy-start(bf16[1,128,4,128]{3,2,1,0:T(4,128)(2,1)} %param.6) | copy-start | bytes 393220
  16.3 0.9 %copy-start.2 = (bf16[1,128,4,128]{3,2,1,0:T(4,128)(2,1)S(1)}, bf16[1,128,4,128]{3,2,1,0:T(4,128)(2,1)}, u32[]{:S(2)}) copy-start(bf16[1,128,4,128]{3,2,1,0:T(4,128)(2,1)} %param.7) | copy-start | bytes 393220
  20.3 0.7 %copy-start.3 = (f32[128]{0:T(128)S(1)}, f32[128]{0:T(128)}, u32[]{:S(2)}) copy-start(f32[128]{0:T(128)} %param.9) | copy-start | bytes 1540

commit v2 on v1

v2 whole, which is shorter than its diff:
```python
import functools
import math

import jax
import jax.numpy as jnp
from jax import lax
from jax.experimental import pallas as pl
from jax.experimental.pallas import tpu as pltpu
from jax.sharding import PartitionSpec as P

QK = 64
SEGMENT = 64
CORES = 2
EXP_SCALE = math.log2(math.e) * QK ** (-0.5)
SPARE_BYTES = 2 << 20
NT = (((1,), (1,)), ((), ()))


def each_head(heads, body):
    if heads <= 8:
        for head in range(heads):
            body(head)
    else:
        lax.fori_loop(0, heads, lambda head, c: (body(head), c)[1], 0)


def sources(peers):
    here = lax.axis_index("sp")
    cores = CORES if peers % CORES == 0 else 1
    chips = peers // cores
    chip, core = here // cores, here % cores
    straight = [lax.rem(chip + chips - r, chips) * cores + core for r in range(chips)]
    crossed = [lax.rem(chip + chips - r, chips) * cores + cores - 1 - core for r in range(chips)]
    if cores == 1:
        return here, [here], straight[1:], []
    return here, [here, crossed[0]], straight[1:], crossed[1:]


def widen(refs, wide):
    for i, ref in enumerate(refs):
        wide[i] = ref[...].astype(jnp.float32)
    return [wide.at[i] for i in range(len(refs))]


def split_rows(ref, head, heads, tokens):
    return ref[pl.ds(head, tokens, stride=heads), :].astype(jnp.bfloat16)


def head_rows(ref, head, tokens):
    return ref[pl.ds(head * tokens, tokens), :]


def hide(scores, here, source, tokens):
    queries = here * tokens + lax.rem(lax.broadcasted_iota(jnp.int32, scores.shape, 0), tokens)
    keys = source * tokens + lax.broadcasted_iota(jnp.int32, scores.shape, 1)
    return jnp.where(keys // SEGMENT <= queries // SEGMENT, scores, -jnp.inf)


def weigh(stacked, keys, srcs, here, tokens, floor):
    scores = [
        hide(lax.dot_general(stacked, key, NT, preferred_element_type=jnp.float32), here, source, tokens)
        for key, source in zip(keys, srcs)
    ]
    top = jnp.max(functools.reduce(jnp.maximum, scores), axis=1, keepdims=True)
    top = jnp.broadcast_to(top, scores[0].shape)
    if floor is not None:
        top = jnp.maximum(top, floor)
    raised = [jnp.exp2((block - top) * EXP_SCALE) for block in scores]
    total = jnp.sum(functools.reduce(jnp.add, raised), axis=1, keepdims=True)
    return top, raised, jnp.broadcast_to(total, scores[0].shape)


def weighted(blocks, values):
    return functools.reduce(
        jnp.add, [jnp.dot(block, value, preferred_element_type=jnp.float32) for block, value in zip(blocks, values)]
    )


def spread(map_weight, tile):
    for own in range(tile.shape[0]):
        tile[own] = jnp.full(tile.shape[1:], map_weight[own])


def prepare(heads, tokens, query, key, value, gain, stacked, key_heads, value_heads, gain_tile, wide):
    query_wide, key_wide, value_wide = widen((query, key, value), wide)

    def body(head):
        rows = split_rows(query_wide, head, heads, tokens)
        first = lax.broadcasted_iota(jnp.int32, rows.shape, 1) < QK
        zero = jnp.zeros_like(rows)
        stacked[head] = jnp.concatenate([jnp.where(first, rows, zero), jnp.where(first, zero, rows)], axis=0)
        key_heads[pl.ds(head * tokens, tokens), :] = split_rows(key_wide, head, heads, tokens)
        value_heads[pl.ds(head * tokens, tokens), :] = split_rows(value_wide, head, heads, tokens)

    each_head(heads, body)
    gain_tile[...] = jnp.broadcast_to(gain[...], gain_tile.shape)


def near_scores(peers, heads, tokens, stacked, key_heads, *refs):
    keys, (raised, top, total, wide) = refs[:-4], refs[-4:]
    here, near, _, _ = sources(peers)
    keys_wide = widen(keys, wide)

    def body(head):
        blocks = [head_rows(key_heads, head, tokens)] + [split_rows(ref, head, heads, tokens) for ref in keys_wide]
        top[head], blocks, total[head] = weigh(stacked[head], blocks, near, here, tokens, None)
        for i, block in enumerate(blocks):
            raised[i, head] = block.astype(jnp.bfloat16)

    each_head(heads, body)


def straight_scores(peers, heads, tokens, counts, stacked, near_raised, floor, value_heads, *refs):
    here, _, straight, _ = sources(peers)
    n_side, n_near = counts
    values, keys = refs[:n_side], refs[n_side:-6]
    raised, top, total, summed, wide, value_wide = refs[-6:]
    keys_wide = widen(keys, wide)
    values_wide = widen(values, value_wide)

    def body(head):
        blocks = [split_rows(ref, head, heads, tokens) for ref in keys_wide]
        top[head], blocks, total[head] = weigh(stacked[head], blocks, straight, here, tokens, floor[head])
        for i, block in enumerate(blocks):
            raised[i, head] = block.astype(jnp.bfloat16)
        near_values = [head_rows(value_heads, head, tokens)] + [split_rows(v, head, heads, tokens) for v in values_wide]
        summed[head] = weighted([near_raised[i, head] for i in range(n_near)], near_values)

    each_head(heads, body)


def last_scores(peers, heads, tokens, stacked, summed, near_top, near_total, far_raised, far_top, far_total, *refs):
    here, _, straight, crossed = sources(peers)
    values, keys = refs[: len(straight)], refs[len(straight) : -4]
    weights, partial, wide, value_wide = refs[-4:]
    keys_wide = widen(keys, wide)
    values_wide = widen(values, value_wide)

    def body(head):
        blocks = [split_rows(ref, head, heads, tokens) for ref in keys_wide]
        peak, blocks, mass = weigh(stacked[head], blocks, crossed, here, tokens, far_top[head])
        near_scale = jnp.exp2((near_top[head] - peak) * EXP_SCALE)
        far_scale = jnp.exp2((far_top[head] - peak) * EXP_SCALE)
        inverse = 1.0 / (near_scale * near_total[head] + far_scale * far_total[head] + mass)
        for i, block in enumerate(blocks):
            weights[i, head] = (block * inverse).astype(jnp.bfloat16)
        far_values = [split_rows(v, head, heads, tokens) for v in values_wide]
        far = weighted([far_raised[i, head] for i in range(len(straight))], far_values)
        partial[head] = (summed[head] * near_scale + far * far_scale) * inverse

    each_head(heads, body)


def write_rows(attended, head, heads, tokens, gain, out_wide):
    mean_square = jnp.mean(attended * attended, axis=1, keepdims=True)
    out_wide[pl.ds(head, tokens, stride=heads), :] = attended * lax.rsqrt(mean_square + 1e-06) * gain[0:1, :]


def owned(head, per_peer, tiles, order):
    second = jnp.zeros((1, tiles[0].shape[-1]), jnp.float32)
    for tile, source in zip(tiles, order):
        for own in range(per_peer):
            second += jnp.where(source * per_peer + own == head, tile[own, 0:1, :], 0.0)
    return second


def finish(peers, heads, tokens, weights, partial, gain, *refs):
    _, near, straight, crossed = sources(peers)
    order = near + straight + crossed
    tiles, values, (out, wide, out_wide) = refs[: len(order)], refs[len(order) : -3], refs[-3:]
    values_wide = widen(values, wide)

    def body(head):
        both = partial[head] + weighted(
            [weights[i, head] for i in range(len(values))], [split_rows(v, head, heads, tokens) for v in values_wide]
        )
        attended = both[:tokens] - owned(head, heads // peers, tiles, order) * both[tokens:]
        write_rows(attended, head, heads, tokens, gain, out_wide)

    each_head(heads, body)
    out[...] = out_wide[...].astype(out.dtype)


def kernel(body, outs, scratch, fetched=False):
    space = pl.BlockSpec(memory_space=pltpu.VMEM)
    held = sum(4 * math.prod(s.shape) for s in scratch)
    held += sum(math.prod(o.shape) * o.dtype.itemsize for o in jax.tree.leaves(outs))
    place = pltpu.HBM if fetched else pltpu.VMEM

    def call(*args):
        scalar = [a.ndim == 1 for a in args]
        limit = SPARE_BYTES + held
        if fetched:
            limit += sum(a.size * a.dtype.itemsize for a in args)
        args = [a if s else pltpu.with_memory_space_constraint(a, place) for a, s in zip(args, scalar)]
        return pl.pallas_call(
            body,
            out_shape=outs,
            in_specs=[pl.BlockSpec(memory_space=pltpu.SMEM) if s else space for s in scalar],
            out_specs=jax.tree.map(lambda _: space, outs),
            scratch_shapes=scratch,
            compiler_params=pltpu.CompilerParams(vmem_limit_bytes=limit),
        )(*args)

    return call


def on_device(query_rows, key_rows, value_rows, map_weight, head_gain):
    peers = lax.axis_size("sp")
    _, tokens, heads, width = query_rows.shape
    cores = CORES if peers % CORES == 0 else 1
    chips = peers // cores
    rows = tokens * heads

    def turn(x, by):
        return lax.ppermute(x, "sp", [(i, (i + by * cores) % peers) for i in range(peers)])

    def swap(x):
        return lax.ppermute(x, "sp", [(i, i // cores * cores + cores - 1 - i % cores) for i in range(peers)])

    def flat(x):
        return x.reshape(rows, width)

    f32 = lambda *s: jax.ShapeDtypeStruct(s, jnp.float32)
    bf16 = lambda *s: jax.ShapeDtypeStruct(s, jnp.bfloat16)
    wide = lambda n: pltpu.VMEM((n, rows, width), jnp.float32)
    both = (heads, 2 * tokens, tokens)
    shift = range(1, chips)
    n_near, n_far, n_last = cores, chips - 1, (chips - 1) * (cores - 1)

    key_far = [turn(key_rows, r) for r in shift]
    tile = kernel(spread, f32(heads // peers, 8, width), [])(map_weight)
    value_far = [turn(value_rows, r) for r in shift]
    weight_far = [turn(tile, r) for r in shift]
    key_near = [swap(key_rows)] if cores > 1 else []
    value_near = [swap(value_rows)] if cores > 1 else []
    weight_near = [tile] + ([swap(tile)] if cores > 1 else [])
    stacked, key_heads, value_heads, gain_tile = kernel(
        functools.partial(prepare, heads, tokens),
        (bf16(heads, 2 * tokens, width), bf16(rows, width), bf16(rows, width), f32(8, width)),
        [wide(3)],
        fetched=True,
    )(flat(query_rows), flat(key_rows), flat(value_rows), head_gain.reshape(1, -1))
    near_raised, near_top, near_total = kernel(
        functools.partial(near_scores, peers, heads, tokens),
        (bf16(n_near, *both), f32(*both), f32(*both)),
        [wide(max(cores - 1, 1))],
    )(stacked, key_heads, *map(flat, key_near))
    key_last = [swap(x) for x in key_far] if cores > 1 else []
    far_raised, far_top, far_total, summed = kernel(
        functools.partial(straight_scores, peers, heads, tokens, (cores - 1, n_near)),
        (bf16(n_far, *both), f32(*both), f32(*both), f32(heads, 2 * tokens, width)),
        [wide(n_far), wide(max(cores - 1, 1))],
    )(stacked, near_raised, near_top, value_heads, *map(flat, value_near), *map(flat, key_far))
    value_last = [swap(x) for x in value_far] if cores > 1 else []
    weight_last = [swap(x) for x in weight_far] if cores > 1 else []
    weights, partial = kernel(
        functools.partial(last_scores, peers, heads, tokens),
        (bf16(n_last, *both), f32(heads, 2 * tokens, width)),
        [wide(n_last), wide(n_far)],
    )(
        stacked, summed, near_top, near_total, far_raised, far_top, far_total,
        *map(flat, value_far), *map(flat, key_last),
    )
    mixed = kernel(
        functools.partial(finish, peers, heads, tokens),
        bf16(rows, width),
        [wide(n_last), pltpu.VMEM((rows, width), jnp.float32)],
    )(weights, partial, gain_tile, *weight_near, *weight_far, *weight_last, *map(flat, value_last))
    return mixed.reshape(query_rows.shape)


def solution(mesh):
    rows = P("dp", "sp", None, None)

    return jax.shard_map(
        on_device,
        mesh=mesh,
        in_specs=(rows, rows, rows, P("sp"), P()),
        out_specs=rows,
        check_vma=False,
    )
```

time: 22.2 us -> 18.6 us (0.84)
  local copies, waits for them, and re-layouts: 2.78 us -> 0 us
  Pallas kernels: 5.27 us -> 3.99 us
  waiting for transfers between devices: 7.37 us -> 7.85 us
    unnamed x8 -> x0, local copies, waits for them, and re-layouts: 2.78 us -> none
    pallas_call x4 -> x6, Pallas kernels: 5.27 us -> 3.99 us  [call(): pl.pallas_call(body, out_shape=outs, in_specs=[pl.BlockSpec(memory_space=...]
    ppermute x3, waiting for transfers between devices: 7.35 us -> 7.84 us  [turn(): lax.ppermute(x, 'sp', [(i, (i + by * cores) % peers) for i in range(peers)])]
  transfers between devices with their start and end apart: 9 -> 9, of which waited for: 3 -> 3; matrix products, arithmetic and copies ran while one was open for 0% -> 0% of each run, Pallas kernels for 20% -> 16%
where the time goes in v2:
time: 18.6 us; the launch traced here: 18.4 us
  waiting for transfers between devices  7.85 us (42%)
  starting transfers between devices  5.85 us (31%)
  Pallas kernels  3.99 us (21%)
  between operations  0.72 us (4%)
    ppermute x3, waiting for transfers between devices, turn(): lax.ppermute(x, 'sp', [(i, (i + by * cores) % peers) for i in range(peers)])  7.84 us
    ppermute x3, starting transfers between devices, turn(): lax.ppermute(x, 'sp', [(i, (i + by * cores) % peers) for i in range(peers)])  4.83 us
    pallas_call x6, Pallas kernels, call(): pl.pallas_call(body, out_shape=outs, in_specs=[pl.BlockSpec(memory_space=...  3.99 us
    ppermute x6, starting transfers between devices, swap(): lax.ppermute(x, 'sp', [(i, i // cores * cores + cores - 1 - i % cores) fo...  1.03 us
  transfers between devices with their start and end apart: 9, of which 3 were waited for; matrix products, arithmetic and copies ran while one was open for 0% of the time, Pallas kernels for 16%

profile of v2, /device:TPU:0, one launch (start us, length us, event | category | flops | bytes accessed | tf_op | source)
XLA Modules:
  0.0 18.4 jit_solution(7541940467207341960)
XLA Ops:
  0.0 3.0 %collective-permute-start.2 = (bf16[1,128,4,128]{3,2,1,0:T(4,128)(2,1)}, bf16[1,128,4,128]{3,2,1,0:T(4,128)(2,1)S(1)}, u32[]{:S(2)}, u32[]{:S(2)}) collective-permute-start(bf16[1,128,4,128]{3,2,1,0:T(4,128)(2,1)} %param.6), channel_id=1, source_target_pairs={{0,16},{8,24},{16,0},{24,8},{1,17},{9,25},{17,1},{25,9},{2,18},{10... | collective-permute-start | bytes 393224 | tf_op jit(solution)/shard_map/ppermute | solution.py:216
  3.0 0.0 collective-permute-start.3
  3.0 0.0 collective-permute-start
  3.0 0.5 %collective-permute-start.1 = (bf16[1,128,4,128]{3,2,1,0:T(4,128)(2,1)}, bf16[1,128,4,128]{3,2,1,0:T(4,128)(2,1)S(1)}, u32[]{:S(2)}, u32[]{:S(2)}) collective-permute-start(bf16[1,128,4,128]{3,2,1,0:T(4,128)(2,1)} %param.7), channel_id=1, source_target_pairs={{0,8},{8,0},{16,24},{24,16},{1,9},{9,1},{17,25},{25,17},{2,10},{10... | collective-permute-start | bytes 393224 | tf_op jit(solution)/shard_map/ppermute | solution.py:219
  3.5 4.0 %collective-permute-done.2 = bf16[1,128,4,128]{3,2,1,0:T(4,128)(2,1)S(1)} collective-permute-done((bf16[1,128,4,128]{3,2,1,0:T(4,128)(2,1)}, bf16[1,128,4,128]{3,2,1,0:T(4,128)(2,1)S(1)}, u32[]{:S(2)}, u32[]{:S(2)}) %collective-permute-start.2) | collective-permute-done | bytes 131104 | tf_op jit(solution)/shard_map/ppermute | solution.py:216
  7.6 0.0 collective-permute-start.4
  7.6 2.0 %collective-permute-done.3 = bf16[1,128,4,128]{3,2,1,0:T(4,128)(2,1)S(1)} collective-permute-done((bf16[1,128,4,128]{3,2,1,0:T(4,128)(2,1)}, bf16[1,128,4,128]{3,2,1,0:T(4,128)(2,1)S(1)}, u32[]{:S(2)}, u32[]{:S(2)}) %collective-permute-start.3) | collective-permute-done | bytes 131104 | tf_op jit(solution)/shard_map/ppermute | solution.py:216
  9.5 0.0 collective-permute-start.8
  10.2 1.8 %collective-permute-start.6 = (f32[1,8,128]{2,1,0:T(8,128)S(1)}, f32[1,8,128]{2,1,0:T(8,128)S(1)}, u32[]{:S(2)}, u32[]{:S(2)}) collective-permute-start(f32[1,8,128]{2,1,0:T(8,128)S(1)} %shard_map.59.refs_0_), channel_id=1, source_target_pairs={{0,16},{8,24},{16,0},{24,8},{1,17},{9,25},{17,1},{25,9},{2,18},{10... | collective-permute-start | bytes 12296 | tf_op jit(solution)/shard_map/ppermute | solution.py:216
  12.0 1.9 %collective-permute-done.6.refs_2_ = f32[1,8,128]{2,1,0:T(8,128)S(1)} collective-permute-done((f32[1,8,128]{2,1,0:T(8,128)S(1)}, f32[1,8,128]{2,1,0:T(8,128)S(1)}, u32[]{:S(2)}, u32[]{:S(2)}) %collective-permute-start.6) | collective-permute-done | bytes 4128 | tf_op jit(solution)/shard_map/ppermute | solution.py:216
  13.8 0.0 collective-permute-start.5
  13.9 0.0 collective-permute-done
  13.9 0.5 %collective-permute-start.7 = (f32[1,8,128]{2,1,0:T(8,128)S(1)}, f32[1,8,128]{2,1,0:T(8,128)S(1)}, u32[]{:S(2)}, u32[]{:S(2)}) collective-permute-start(f32[1,8,128]{2,1,0:T(8,128)S(1)} %collective-permute-done.6.refs_2_), channel_id=1, source_target_pairs={{0,8},{8,0},{16,24},{24,16},{1,9},{9,1},{17,25},{25,17},{2,10},{10... | collective-permute-start | bytes 12296 | tf_op jit(solution)/shard_map/ppermute | solution.py:219
  14.4 1.1 %shard_map.55 = (bf16[4,256,128]{2,1,0:T(8,128)(2,1)S(1)}, bf16[512,128]{1,0:T(8,128)(2,1)S(1)}, bf16[512,128]{1,0:T(8,128)(2,1)S(1)}, f32[8,128]{1,0:T(8,128)S(1)}) custom-call(bf16[512,128]{1,0:T(8,128)(2,1)} %bitcast.17, bf16[512,128]{1,0:T(8,128)(2,1)} %bitcast.18, bf16[512,128]{1,0:T(8,128)(2,1)} %bitcast.19, f32[1,128]{1,0:T(1,128)} %bitcast.20), custom_call_target="tpu_custom_call" | custom-call | tf_op jit(solution)/shard_map/pallas_call | solution.py:196
  15.5 0.6 %shard_map.56 = (bf16[2,4,256,128]{3,2,1,0:T(8,128)(2,1)S(1)}, f32[4,256,128]{2,1,0:T(8,128)S(1)}, f32[4,256,128]{2,1,0:T(8,128)S(1)}) custom-call(bf16[4,256,128]{2,1,0:T(8,128)(2,1)S(1)} %get-tuple-element.18.stacked, bf16[512,128]{1,0:T(8,128)(2,1)S(1)} %get-tuple-element.19.key_heads, bf16[512,128]{1,0:T(8,128)(2,1)S(1)} %bitcast.11), custom_call_target="tpu_custom_call" | custom-call | tf_op jit(solution)/shard_map/pallas_call | solution.py:196
  16.1 0.0 collective-permute-done.1
  16.1 0.6 %shard_map.57 = (bf16[1,4,256,128]{3,2,1,0:T(8,128)(2,1)S(1)}, f32[4,256,128]{2,1,0:T(8,128)S(1)}, f32[4,256,128]{2,1,0:T(8,128)S(1)}, f32[4,256,128]{2,1,0:T(8,128)S(1)}) custom-call(bf16[4,256,128]{2,1,0:T(8,128)(2,1)S(1)} %get-tuple-element.18.stacked, bf16[2,4,256,128]{3,2,1,0:T(8,128)(2,1)S(1)} %get-tuple-element.20.near_raised, ...), custom_call_target="tpu_custom_call" | custom-call | tf_op jit(solution)/shard_map/pallas_call | solution.py:196
  16.7 0.0 collective-permute-done.4
  16.7 0.7 %shard_map.58 = (bf16[1,4,256,128]{3,2,1,0:T(8,128)(2,1)S(1)}, f32[4,256,128]{2,1,0:T(8,128)S(1)}) custom-call(bf16[4,256,128]{2,1,0:T(8,128)(2,1)S(1)} %get-tuple-element.18.stacked, f32[4,256,128]{2,1,0:T(8,128)S(1)} %get-tuple-element.23.summed, f32[4,256,128]{2,1,0:T(8,128)S(1)} %get-tuple-element.21.floor.near_top, ...), custom_call_target="tpu_custom_call" | custom-call | tf_op jit(solution)/shard_map/pallas_call | solution.py:196
  17.4 0.0 collective-permute-done.5.refs_1_
  17.4 0.0 collective-permute-done.7.refs_3_
  17.4 0.0 collective-permute-done.8
  17.4 1.0 %shard_map.60 = bf16[512,128]{1,0:T(8,128)(2,1)} custom-call(bf16[1,4,256,128]{3,2,1,0:T(8,128)(2,1)S(1)} %get-tuple-element.28.weights, f32[4,256,128]{2,1,0:T(8,128)S(1)} %get-tuple-element.29.partial, f32[8,128]{1,0:T(8,128)S(1)} %get-tuple-element.30.gain, f32[1,8,128]{2,1,0:T(8,128)S(1)} %shard_map.59.refs_0_, ...), custom_call_target="tpu_custom_call" | custom-call | tf_op jit(solution)/shard_map/pallas_call | solution.py:196
  (1 shorter events, 0.0 us)
Async XLA Ops:
  0.0 7.5 %collective-permute-start.2 = (bf16[1,128,4,128]{3,2,1,0:T(4,128)(2,1)}, bf16[1,128,4,128]{3,2,1,0:T(4,128)(2,1)S(1)}, u32[]{:S(2)}, u32[]{:S(2)}) collective-permute-start(bf16[1,128,4,128]{3,2,1,0:T(4,128)(2,1)} %param.6), channel_id=1, source_target_pairs={{0,16},{8,24},{16,0},{24,8},{1,17},{9,25},{17,1},{25,9},{2,18},{10... | collective-permute-start | bytes 393224 | tf_op jit(solution)/shard_map/ppermute | solution.py:216
  3.0 6.5 %collective-permute-start.3 = (bf16[1,128,4,128]{3,2,1,0:T(4,128)(2,1)}, bf16[1,128,4,128]{3,2,1,0:T(4,128)(2,1)S(1)}, u32[]{:S(2)}, u32[]{:S(2)}) collective-permute-start(bf16[1,128,4,128]{3,2,1,0:T(4,128)(2,1)} %param.7), channel_id=1, source_target_pairs={{0,16},{8,24},{16,0},{24,8},{1,17},{9,25},{17,1},{25,9},{2,18},{10... | collective-permute-start | bytes 393224 | tf_op jit(solution)/shard_map/ppermute | solution.py:216
  3.0 10.8 %collective-permute-start = (bf16[1,128,4,128]{3,2,1,0:T(4,128)(2,1)}, bf16[1,128,4,128]{3,2,1,0:T(4,128)(2,1)S(1)}, u32[]{:S(2)}, u32[]{:S(2)}) collective-permute-start(bf16[1,128,4,128]{3,2,1,0:T(4,128)(2,1)} %param.6), channel_id=1, source_target_pairs={{0,8},{8,0},{16,24},{24,16},{1,9},{9,1},{17,25},{25,17},{2,10},{10... | collective-permute-start | bytes 393224 | tf_op jit(solution)/shard_map/ppermute | solution.py:219
  3.0 13.1 %collective-permute-start.1 = (bf16[1,128,4,128]{3,2,1,0:T(4,128)(2,1)}, bf16[1,128,4,128]{3,2,1,0:T(4,128)(2,1)S(1)}, u32[]{:S(2)}, u32[]{:S(2)}) collective-permute-start(bf16[1,128,4,128]{3,2,1,0:T(4,128)(2,1)} %param.7), channel_id=1, source_target_pairs={{0,8},{8,0},{16,24},{24,16},{1,9},{9,1},{17,25},{25,17},{2,10},{10... | collective-permute-start | bytes 393224 | tf_op jit(solution)/shard_map/ppermute | solution.py:219
  7.6 9.1 %collective-permute-start.4 = (bf16[1,128,4,128]{3,2,1,0:T(4,128)(2,1)S(1)}, bf16[1,128,4,128]{3,2,1,0:T(4,128)(2,1)S(1)}, u32[]{:S(2)}, u32[]{:S(2)}) collective-permute-start(bf16[1,128,4,128]{3,2,1,0:T(4,128)(2,1)S(1)} %collective-permute-done.2), channel_id=1, source_target_pairs={{0,8},{8,0},{16,24},{24,16},{1,9},{9,1},{17,25},{25,17},{2,10},{10... | collective-permute-start | bytes 393224 | tf_op jit(solution)/shard_map/ppermute | solution.py:219
  9.5 7.9 %collective-permute-start.8 = (bf16[1,128,4,128]{3,2,1,0:T(4,128)(2,1)S(1)}, bf16[1,128,4,128]{3,2,1,0:T(4,128)(2,1)S(1)}, u32[]{:S(2)}, u32[]{:S(2)}) collective-permute-start(bf16[1,128,4,128]{3,2,1,0:T(4,128)(2,1)S(1)} %collective-permute-done.3), channel_id=1, source_target_pairs={{0,8},{8,0},{16,24},{24,16},{1,9},{9,1},{17,25},{25,17},{2,10},{10... | collective-permute-start | bytes 393224 | tf_op jit(solution)/shard_map/ppermute | solution.py:219
  10.2 3.7 %collective-permute-start.6 = (f32[1,8,128]{2,1,0:T(8,128)S(1)}, f32[1,8,128]{2,1,0:T(8,128)S(1)}, u32[]{:S(2)}, u32[]{:S(2)}) collective-permute-start(f32[1,8,128]{2,1,0:T(8,128)S(1)} %shard_map.59.refs_0_), channel_id=1, source_target_pairs={{0,16},{8,24},{16,0},{24,8},{1,17},{9,25},{17,1},{25,9},{2,18},{10... | collective-permute-start | bytes 12296 | tf_op jit(solution)/shard_map/ppermute | solution.py:216
  13.8 3.5 %collective-permute-start.5 = (f32[1,8,128]{2,1,0:T(8,128)S(1)}, f32[1,8,128]{2,1,0:T(8,128)S(1)}, u32[]{:S(2)}, u32[]{:S(2)}) collective-permute-start(f32[1,8,128]{2,1,0:T(8,128)S(1)} %shard_map.59.refs_0_), channel_id=1, source_target_pairs={{0,8},{8,0},{16,24},{24,16},{1,9},{9,1},{17,25},{25,17},{2,10},{10... | collective-permute-start | bytes 12296 | tf_op jit(solution)/shard_map/ppermute | solution.py:219
  13.9 3.5 %collective-permute-start.7 = (f32[1,8,128]{2,1,0:T(8,128)S(1)}, f32[1,8,128]{2,1,0:T(8,128)S(1)}, u32[]{:S(2)}, u32[]{:S(2)}) collective-permute-start(f32[1,8,128]{2,1,0:T(8,128)S(1)} %collective-permute-done.6.refs_2_), channel_id=1, source_target_pairs={{0,8},{8,0},{16,24},{24,16},{1,9},{9,1},{17,25},{25,17},{2,10},{10... | collective-permute-start | bytes 12296 | tf_op jit(solution)/shard_map/ppermute | solution.py:219

commit v3 on v2

--- a/solution.py
+++ b/solution.py
@@ -76,11 +76,6 @@
     )
 
 
-def spread(map_weight, tile):
-    for own in range(tile.shape[0]):
-        tile[own] = jnp.full(tile.shape[1:], map_weight[own])
-
-
 def prepare(heads, tokens, query, key, value, gain, stacked, key_heads, value_heads, gain_tile, wide):
     query_wide, key_wide, value_wide = widen((query, key, value), wide)
 
@@ -96,10 +91,14 @@
     gain_tile[...] = jnp.broadcast_to(gain[...], gain_tile.shape)
 
 
-def near_scores(peers, heads, tokens, stacked, key_heads, *refs):
-    keys, (raised, top, total, wide) = refs[:-4], refs[-4:]
+def near_scores(peers, heads, tokens, stacked, key_heads, gain, *refs):
     here, near, _, _ = sources(peers)
+    tiles, keys = refs[: len(near)], refs[len(near) : -6]
+    raised, top, total, gain_out, pair, wide = refs[-6:]
     keys_wide = widen(keys, wide)
+    gain_out[...] = gain[...]
+    for i, tile in enumerate(tiles):
+        pair[i] = tile[...]
 
     def body(head):
         blocks = [head_rows(key_heads, head, tokens)] + [split_rows(ref, head, heads, tokens) for ref in keys_wide]
@@ -110,11 +109,13 @@
     each_head(heads, body)
 
 
-def straight_scores(peers, heads, tokens, counts, stacked, near_raised, floor, value_heads, *refs):
+def straight_scores(peers, heads, tokens, counts, stacked, near_raised, floor, gain, pair, value_heads, *refs):
     here, _, straight, _ = sources(peers)
     n_side, n_near = counts
-    values, keys = refs[:n_side], refs[n_side:-6]
-    raised, top, total, summed, wide, value_wide = refs[-6:]
+    values, keys = refs[:n_side], refs[n_side:-8]
+    raised, top, total, summed, gain_out, pair_out, wide, value_wide = refs[-8:]
+    gain_out[...] = gain[...]
+    pair_out[...] = pair[...]
     keys_wide = widen(keys, wide)
     values_wide = widen(values, value_wide)
 
@@ -127,6 +128,18 @@
         summed[head] = weighted([near_raised[i, head] for i in range(n_near)], near_values)
 
     each_head(heads, body)
+
+
+def owned(head, per_peer, pairs, order):
+    near, straight, crossed = order
+    owners = [(pairs[0], i, source) for i, source in enumerate(near)]
+    for pair, *both in zip(pairs[1:], straight, *([crossed] if crossed else [])):
+        owners += [(pair, i, source) for i, source in enumerate(both)]
+    second = jnp.zeros((1, pairs[0].shape[-1]), jnp.float32)
+    for ref, i, source in owners:
+        for own in range(per_peer):
+            second += jnp.where(source * per_peer + own == head, ref[i, own, 0:1, :], 0.0)
+    return second
 
 
 def last_scores(peers, heads, tokens, stacked, summed, near_top, near_total, far_raised, far_top, far_total, *refs):
@@ -156,49 +169,63 @@
     out_wide[pl.ds(head, tokens, stride=heads), :] = attended * lax.rsqrt(mean_square + 1e-06) * gain[0:1, :]
 
 
-def owned(head, per_peer, tiles, order):
-    second = jnp.zeros((1, tiles[0].shape[-1]), jnp.float32)
-    for tile, source in zip(tiles, order):
-        for own in range(per_peer):
-            second += jnp.where(source * per_peer + own == head, tile[own, 0:1, :], 0.0)
-    return second
+def finish_near(peers, heads, tokens, summed, near_total, gain, *refs):
+    pairs, (out, out_wide) = refs[:-2], refs[-2:]
+    order = sources(peers)[1:]
+
+    def body(head):
+        both = summed[head] / near_total[head]
+        attended = both[:tokens] - owned(head, heads // peers, pairs, order) * both[tokens:]
+        write_rows(attended, head, heads, tokens, gain, out_wide)
+
+    each_head(heads, body)
+    out[...] = out_wide[...].astype(out.dtype)
 
 
 def finish(peers, heads, tokens, weights, partial, gain, *refs):
-    _, near, straight, crossed = sources(peers)
-    order = near + straight + crossed
-    tiles, values, (out, wide, out_wide) = refs[: len(order)], refs[len(order) : -3], refs[-3:]
+    order = sources(peers)[1:]
+    n_pairs = 1 + len(order[1])
+    pairs, values, (out, wide, out_wide) = refs[:n_pairs], refs[n_pairs:-3], refs[-3:]
     values_wide = widen(values, wide)
 
     def body(head):
         both = partial[head] + weighted(
             [weights[i, head] for i in range(len(values))], [split_rows(v, head, heads, tokens) for v in values_wide]
         )
-        attended = both[:tokens] - owned(head, heads // peers, tiles, order) * both[tokens:]
+        attended = both[:tokens] - owned(head, heads // peers, pairs, order) * both[tokens:]
         write_rows(attended, head, heads, tokens, gain, out_wide)
 
     each_head(heads, body)
     out[...] = out_wide[...].astype(out.dtype)
 
 
-def kernel(body, outs, scratch, fetched=False):
+def spread(map_weight, tile):
+    for own in range(tile.shape[0]):
+        tile[own] = jnp.full(tile.shape[1:], map_weight[own])
+
+
+def hold(*refs):
+    pass
+
+
+def kernel(body, outs, scratch, fetched=False, keep=False):
     space = pl.BlockSpec(memory_space=pltpu.VMEM)
-    held = sum(4 * math.prod(s.shape) for s in scratch)
+    held = sum(4 * math.prod(s.shape) for s in scratch if s.dtype == jnp.float32)
     held += sum(math.prod(o.shape) * o.dtype.itemsize for o in jax.tree.leaves(outs))
-    place = pltpu.HBM if fetched else pltpu.VMEM
 
     def call(*args):
-        scalar = [a.ndim == 1 for a in args]
         limit = SPARE_BYTES + held
         if fetched:
             limit += sum(a.size * a.dtype.itemsize for a in args)
-        args = [a if s else pltpu.with_memory_space_constraint(a, place) for a, s in zip(args, scalar)]
+        if fetched or keep:
+            args = [pltpu.with_memory_space_constraint(a, pltpu.HBM if fetched else pltpu.VMEM) for a in args]
         return pl.pallas_call(
             body,
             out_shape=outs,
-            in_specs=[pl.BlockSpec(memory_space=pltpu.SMEM) if s else space for s in scalar],
+            in_specs=[pl.BlockSpec(memory_space=pltpu.SMEM) if a.ndim == 1 else space for a in args],
             out_specs=jax.tree.map(lambda _: space, outs),
             scratch_shapes=scratch,
+            input_output_aliases={i: i for i in range(len(args))} if keep else {},
             compiler_params=pltpu.CompilerParams(vmem_limit_bytes=limit),
         )(*args)
 
@@ -229,44 +256,57 @@
     n_near, n_far, n_last = cores, chips - 1, (chips - 1) * (cores - 1)
 
     key_far = [turn(key_rows, r) for r in shift]
+    value_far = [turn(value_rows, r) for r in shift]
     tile = kernel(spread, f32(heads // peers, 8, width), [])(map_weight)
-    value_far = [turn(value_rows, r) for r in shift]
-    weight_far = [turn(tile, r) for r in shift]
+    tiles = [tile] + ([swap(tile)] if cores > 1 else [])
     key_near = [swap(key_rows)] if cores > 1 else []
     value_near = [swap(value_rows)] if cores > 1 else []
-    weight_near = [tile] + ([swap(tile)] if cores > 1 else [])
     stacked, key_heads, value_heads, gain_tile = kernel(
         functools.partial(prepare, heads, tokens),
         (bf16(heads, 2 * tokens, width), bf16(rows, width), bf16(rows, width), f32(8, width)),
         [wide(3)],
         fetched=True,
     )(flat(query_rows), flat(key_rows), flat(value_rows), head_gain.reshape(1, -1))
-    near_raised, near_top, near_total = kernel(
+    near_raised, near_top, near_total, gain_tile, pair = kernel(
         functools.partial(near_scores, peers, heads, tokens),
-        (bf16(n_near, *both), f32(*both), f32(*both)),
+        (bf16(n_near, *both), f32(*both), f32(*both), f32(8, width), f32(n_near, heads // peers, 8, width)),
         [wide(max(cores - 1, 1))],
-    )(stacked, key_heads, *map(flat, key_near))
+    )(stacked, key_heads, gain_tile, *tiles, *map(flat, key_near))
+    pairs = [pair] + [turn(pair, r) for r in shift]
     key_last = [swap(x) for x in key_far] if cores > 1 else []
-    far_raised, far_top, far_total, summed = kernel(
+    far_raised, far_top, far_total, summed, gain_tile, pair_tile = kernel(
         functools.partial(straight_scores, peers, heads, tokens, (cores - 1, n_near)),
-        (bf16(n_far, *both), f32(*both), f32(*both), f32(heads, 2 * tokens, width)),
+        (bf16(n_far, *both), f32(*both), f32(*both), f32(heads, 2 * tokens, width), f32(8, width), f32(*pair.shape)),
         [wide(n_far), wide(max(cores - 1, 1))],
-    )(stacked, near_raised, near_top, value_heads, *map(flat, value_near), *map(flat, key_far))
-    value_last = [swap(x) for x in value_far] if cores > 1 else []
-    weight_last = [swap(x) for x in weight_far] if cores > 1 else []
-    weights, partial = kernel(
-        functools.partial(last_scores, peers, heads, tokens),
-        (bf16(n_last, *both), f32(heads, 2 * tokens, width)),
-        [wide(n_last), wide(n_far)],
-    )(
-        stacked, summed, near_top, near_total, far_raised, far_top, far_total,
-        *map(flat, value_far), *map(flat, key_last),
-    )
-    mixed = kernel(
-        functools.partial(finish, peers, heads, tokens),
-        bf16(rows, width),
-        [wide(n_last), pltpu.VMEM((rows, width), jnp.float32)],
-    )(weights, partial, gain_tile, *weight_near, *weight_far, *weight_last, *map(flat, value_last))
+    )(stacked, near_raised, near_top, gain_tile, pair, value_heads, *map(flat, value_near), *map(flat, key_far))
+    arrived = (*value_far, *key_last, *pairs[1:])
+    arrived = kernel(hold, tuple(jax.ShapeDtypeStruct(x.shape, x.dtype) for x in arrived), [], keep=True)(*arrived)
+    value_far, key_last, pairs = arrived[:n_far], arrived[n_far : n_far + n_last], [pair_tile, *arrived[n_far + n_last :]]
+
+    def later_chip():
+        value_last = [swap(x) for x in value_far] if cores > 1 else []
+        weights, partial = kernel(
+            functools.partial(last_scores, peers, heads, tokens),
+            (bf16(n_last, *both), f32(heads, 2 * tokens, width)),
+            [wide(n_last), wide(n_far)],
+        )(
+            stacked, summed, near_top, near_total, far_raised, far_top, far_total,
+            *map(flat, value_far), *map(flat, key_last),
+        )
+        return kernel(
+            functools.partial(finish, peers, heads, tokens),
+            bf16(rows, width),
+            [wide(n_last), pltpu.VMEM((rows, width), jnp.float32)],
+        )(weights, partial, gain_tile, *pairs, *map(flat, value_last))
+
+    def first_chip():
+        return kernel(
+            functools.partial(finish_near, peers, heads, tokens),
+            bf16(rows, width),
+            [pltpu.VMEM((rows, width), jnp.float32)],
+        )(summed, near_total, gain_tile, *pairs)
+
+    mixed = lax.cond(lax.axis_index("sp") >= cores, later_chip, first_chip)
     return mixed.reshape(query_rows.shape)
 
 

time: 18.6 us -> 16.1 us (0.87)
  the two profiles are of different devices: /device:TPU:0 before, /device:TPU:5 now
where the time goes in v3:
time: 16.1 us; the launch traced here: 16 us
  starting transfers between devices  6.88 us (43%)
  waiting for transfers between devices  4.25 us (26%)
  Pallas kernels  3.46 us (21%)
  between operations  0.74 us (5%)
  local copies, waits for them, and re-layouts  0.65 us (4%)
    ppermute x5, starting transfers between devices, swap(): lax.ppermute(x, 'sp', [(i, i // cores * cores + cores - 1 - i % cores) fo...  5.13 us
    ppermute x3, waiting for transfers between devices, turn(): lax.ppermute(x, 'sp', [(i, (i + by * cores) % peers) for i in range(peers)])  4.04 us
    pallas_call x7, Pallas kernels, call(): pl.pallas_call(body, out_shape=outs, in_specs=[pl.BlockSpec(memory_space=...  3.46 us
    ppermute x3, starting transfers between devices, turn(): lax.ppermute(x, 'sp', [(i, (i + by * cores) % peers) for i in range(peers)])  1.75 us
    unnamed x2, local copies, waits for them, and re-layouts  0.65 us
  transfers between devices with their start and end apart: 8, of which 3 were waited for; matrix products, arithmetic and copies ran while one was open for 0% of the time, Pallas kernels for 19%

profile of v3, /device:TPU:5, one launch (start us, length us, event | category | flops | bytes accessed | tf_op | source)
XLA Modules:
  0.0 16.0 jit_solution(16633041782524605358)
XLA Ops:
  0.0 0.0 collective-permute-start.4
  0.0 0.7 %collective-permute-start.2 = (bf16[1,128,4,128]{3,2,1,0:T(4,128)(2,1)}, bf16[1,128,4,128]{3,2,1,0:T(4,128)(2,1)S(1)}, u32[]{:S(2)}, u32[]{:S(2)}) collective-permute-start(bf16[1,128,4,128]{3,2,1,0:T(4,128)(2,1)} %param.8), channel_id=1, source_target_pairs={{0,8},{8,0},{16,24},{24,16},{1,9},{9,1},{17,25},{25,17},{2,10},{10... | collective-permute-start | bytes 393224 | tf_op jit(solution)/shard_map/ppermute | solution.py:246
  0.7 0.1 collective-permute-start.3
  0.8 1.7 %collective-permute-start.5 = (bf16[1,128,4,128]{3,2,1,0:T(4,128)(2,1)}, bf16[1,128,4,128]{3,2,1,0:T(4,128)(2,1)S(1)}, u32[]{:S(2)}, u32[]{:S(2)}) collective-permute-start(bf16[1,128,4,128]{3,2,1,0:T(4,128)(2,1)} %param.9), channel_id=1, source_target_pairs={{0,16},{8,24},{16,0},{24,8},{1,17},{9,25},{17,1},{25,9},{2,18},{10... | collective-permute-start | bytes 393224 | tf_op jit(solution)/shard_map/ppermute | solution.py:243
  2.4 2.2 %collective-permute-done.4 = bf16[1,128,4,128]{3,2,1,0:T(4,128)(2,1)S(1)} collective-permute-done((bf16[1,128,4,128]{3,2,1,0:T(4,128)(2,1)}, bf16[1,128,4,128]{3,2,1,0:T(4,128)(2,1)S(1)}, u32[]{:S(2)}, u32[]{:S(2)}) %collective-permute-start.4) | collective-permute-done | bytes 131104 | tf_op jit(solution)/shard_map/ppermute | solution.py:243
  4.6 2.7 %collective-permute-start.6 = (bf16[1,128,4,128]{3,2,1,0:T(4,128)(2,1)S(1)}, bf16[1,128,4,128]{3,2,1,0:T(4,128)(2,1)S(1)}, u32[]{:S(2)}, u32[]{:S(2)}) collective-permute-start(bf16[1,128,4,128]{3,2,1,0:T(4,128)(2,1)S(1)} %collective-permute-done.4), channel_id=1, source_target_pairs={{0,8},{8,0},{16,24},{24,16},{1,9},{9,1},{17,25},{25,17},{2,10},{10... | collective-permute-start | bytes 393224 | tf_op jit(solution)/shard_map/ppermute | solution.py:246
  7.9 0.1 collective-permute-start.1
  8.0 1.2 %shard_map.57 = (bf16[4,256,128]{2,1,0:T(8,128)(2,1)S(1)}, bf16[512,128]{1,0:T(8,128)(2,1)S(1)}, bf16[512,128]{1,0:T(8,128)(2,1)S(1)}, f32[8,128]{1,0:T(8,128)S(1)}) custom-call(bf16[512,128]{1,0:T(8,128)(2,1)} %bitcast.20, bf16[512,128]{1,0:T(8,128)(2,1)} %bitcast.21, bf16[512,128]{1,0:T(8,128)(2,1)} %bitcast.22, f32[1,128]{1,0:T(1,128)} %bitcast.23), custom_call_target="tpu_custom_call" | custom-call | tf_op jit(solution)/shard_map/pallas_call | solution.py:222
  9.2 0.0 collective-permute-done.1.refs_1_
  9.2 0.0 collective-permute-done.2
  9.2 0.6 %shard_map.59 = (bf16[2,4,256,128]{3,2,1,0:T(8,128)(2,1)S(1)}, f32[4,256,128]{2,1,0:T(8,128)S(1)}, f32[4,256,128]{2,1,0:T(8,128)S(1)}, f32[8,128]{1,0:T(8,128)S(1)}, f32[2,1,8,128]{3,2,1,0:T(8,128)S(1)}) custom-call(bf16[4,256,128]{2,1,0:T(8,128)(2,1)S(1)} %get-tuple-element.80.stacked, bf16[512,128]{1,0:T(8,128)(2,1)S(1)} %get-tuple-element.81.key_heads, ...), custom_call_target="tpu_custom_call" | custom-call | tf_op jit(solution)/shard_map/pallas_call | solution.py:222
  9.7 0.1 collective-permute-start.7
  9.8 0.0 collective-permute-done.3
  9.8 0.6 %shard_map.60 = (bf16[1,4,256,128]{3,2,1,0:T(8,128)(2,1)S(1)}, f32[4,256,128]{2,1,0:T(8,128)S(1)}, f32[4,256,128]{2,1,0:T(8,128)S(1)}, f32[4,256,128]{2,1,0:T(8,...) custom-call(bf16[4,256,128]{2,1,0:T(8,128)(2,1)S(1)} %get-tuple-element.80.stacked, ...), custom_call_target="tpu_custom_call" | custom-call | tf_op jit(solution)/shard_map/pallas_call | solution.py:222
  10.4 0.0 collective-permute-done.5.refs_0_
  10.4 1.9 %collective-permute-done.7.refs_2_ = f32[2,1,8,128]{3,2,1,0:T(8,128)S(1)} collective-permute-done((f32[2,1,8,128]{3,2,1,0:T(8,128)S(1)}, f32[2,1,8,128]{3,2,1,0:T(8,128)S(1)}, u32[]{:S(2)}, u32[]{:S(2)}) %collective-permute-start.7) | collective-permute-done | bytes 8224 | tf_op jit(solution)/shard_map/ppermute | solution.py:243
  12.3 0.0 collective-permute-done.6.refs_1_
  12.3 3.0 %conditional.1 = (bf16[1,128,4,128]{3,2,1,0:T(4,128)(2,1)S(1)}) conditional(s32[]{:T(128)} %convert_element_type.3, (f32[4,256,128]{2,1,0:T(8,128)S(1)}, f32[4,256,128]{2,1,0:T(8,128)S(1)}, f32[8,128]{1,0:T(8,128)S(1)}, f32[2,1,8,128]{3,2,1,0:T(8,128)S(1)}, f32[2,1,8,128]{3,2,1,0:T(8,128)S(1)}) %tuple.13, (bf16[1,128,4,128]{3,2,1,0:T(4,128)(2,1)S(1)}, ...), branch_computations={%region_0.0_spmd, %region_1.0_spmd} | conditional | bytes 524336 | solution.py:309
  12.3 1.7 %collective-permute-start = (bf16[1,128,4,128]{3,2,1,0:T(4,128)(2,1)S(1)}, bf16[1,128,4,128]{3,2,1,0:T(4,128)(2,1)S(1)}, u32[]{:S(2)}, u32[]{:S(2)}) collective-permute-start(bf16[1,128,4,128]{3,2,1,0:T(4,128)(2,1)S(1)} %get-tuple-element.55), channel_id=1, source_target_pairs={{0,8},{8,0},{16,24},{24,16},{1,9},{9,1},{17,25},{25,17},{2,10},{10... | collective-permute-start | bytes 393224 | tf_op jit(solution)/shard_map/cond/branch_1_fun/ppermute | solution.py:246
  14.0 0.8 %branch_1_fun.2 = (bf16[1,4,256,128]{3,2,1,0:T(8,128)(2,1)S(1)}, f32[4,256,128]{2,1,0:T(8,128)S(1)}) custom-call(bf16[4,256,128]{2,1,0:T(8,128)(2,1)S(1)} %get-tuple-element.48.stacked, f32[4,256,128]{2,1,0:T(8,128)S(1)} %get-tuple-element.49.summed, f32[4,256,128]{2,1,0:T(8,128)S(1)} %get-tuple-element.50.near_top, ...), custom_call_target="tpu_custom_call" | custom-call | tf_op jit(solution)/shard_map/cond/branch_1_fun/pallas_call | solution.py:222
  14.8 0.2 %collective-permute-done = bf16[1,128,4,128]{3,2,1,0:T(4,128)(2,1)S(1)} collective-permute-done((bf16[1,128,4,128]{3,2,1,0:T(4,128)(2,1)S(1)}, bf16[1,128,4,128]{3,2,1,0:T(4,128)(2,1)S(1)}, u32[]{:S(2)}, u32[]{:S(2)}) %collective-permute-start) | collective-permute-done | bytes 131104 | tf_op jit(solution)/shard_map/cond/branch_1_fun/ppermute | solution.py:246
  15.0 0.4 %branch_1_fun.3 = bf16[512,128]{1,0:T(8,128)(2,1)S(1)} custom-call(bf16[1,4,256,128]{3,2,1,0:T(8,128)(2,1)S(1)} %get-tuple-element.57.weights, f32[4,256,128]{2,1,0:T(8,128)S(1)} %get-tuple-element.58.partial, f32[8,128]{1,0:T(8,128)S(1)} %get-tuple-element.59.gain, f32[2,1,8,128]{3,2,1,0:T(8,128)S(1)} %get-tuple-element.60.refs_0_, ...), custom_call_target="tpu_custom_call" | custom-call | tf_op jit(solution)/shard_map/cond/branch_1_fun/pallas_call | solution.py:222
  15.3 0.0 copy-start
  15.3 0.6 %copy-done = bf16[1,128,4,128]{3,2,1,0:T(4,128)(2,1)} copy-done((bf16[1,128,4,128]{3,2,1,0:T(4,128)(2,1)}, bf16[1,128,4,128]{3,2,1,0:T(4,128)(2,1)S(1)}, u32[]{:S(2)}) %copy-start) | copy-done | bytes 131096
  (2 shorter events, 0.0 us)
Async XLA Ops:
  0.0 4.6 %collective-permute-start.4 = (bf16[1,128,4,128]{3,2,1,0:T(4,128)(2,1)}, bf16[1,128,4,128]{3,2,1,0:T(4,128)(2,1)S(1)}, u32[]{:S(2)}, u32[]{:S(2)}) collective-permute-start(bf16[1,128,4,128]{3,2,1,0:T(4,128)(2,1)} %param.8), channel_id=1, source_target_pairs={{0,16},{8,24},{16,0},{24,8},{1,17},{9,25},{17,1},{25,9},{2,18},{10... | collective-permute-start | bytes 393224 | tf_op jit(solution)/shard_map/ppermute | solution.py:243
  0.0 9.2 %collective-permute-start.2 = (bf16[1,128,4,128]{3,2,1,0:T(4,128)(2,1)}, bf16[1,128,4,128]{3,2,1,0:T(4,128)(2,1)S(1)}, u32[]{:S(2)}, u32[]{:S(2)}) collective-permute-start(bf16[1,128,4,128]{3,2,1,0:T(4,128)(2,1)} %param.8), channel_id=1, source_target_pairs={{0,8},{8,0},{16,24},{24,16},{1,9},{9,1},{17,25},{25,17},{2,10},{10... | collective-permute-start | bytes 393224 | tf_op jit(solution)/shard_map/ppermute | solution.py:246
  0.7 9.2 %collective-permute-start.3 = (bf16[1,128,4,128]{3,2,1,0:T(4,128)(2,1)}, bf16[1,128,4,128]{3,2,1,0:T(4,128)(2,1)S(1)}, u32[]{:S(2)}, u32[]{:S(2)}) collective-permute-start(bf16[1,128,4,128]{3,2,1,0:T(4,128)(2,1)} %param.9), channel_id=1, source_target_pairs={{0,8},{8,0},{16,24},{24,16},{1,9},{9,1},{17,25},{25,17},{2,10},{10... | collective-permute-start | bytes 393224 | tf_op jit(solution)/shard_map/ppermute | solution.py:246
  0.8 9.7 %collective-permute-start.5 = (bf16[1,128,4,128]{3,2,1,0:T(4,128)(2,1)}, bf16[1,128,4,128]{3,2,1,0:T(4,128)(2,1)S(1)}, u32[]{:S(2)}, u32[]{:S(2)}) collective-permute-start(bf16[1,128,4,128]{3,2,1,0:T(4,128)(2,1)} %param.9), channel_id=1, source_target_pairs={{0,16},{8,24},{16,0},{24,8},{1,17},{9,25},{17,1},{25,9},{2,18},{10... | collective-permute-start | bytes 393224 | tf_op jit(solution)/shard_map/ppermute | solution.py:243
  4.6 7.7 %collective-permute-start.6 = (bf16[1,128,4,128]{3,2,1,0:T(4,128)(2,1)S(1)}, bf16[1,128,4,128]{3,2,1,0:T(4,128)(2,1)S(1)}, u32[]{:S(2)}, u32[]{:S(2)}) collective-permute-start(bf16[1,128,4,128]{3,2,1,0:T(4,128)(2,1)S(1)} %collective-permute-done.4), channel_id=1, source_target_pairs={{0,8},{8,0},{16,24},{24,16},{1,9},{9,1},{17,25},{25,17},{2,10},{10... | collective-permute-start | bytes 393224 | tf_op jit(solution)/shard_map/ppermute | solution.py:246
  7.9 1.2 %collective-permute-start.1 = (f32[1,8,128]{2,1,0:T(8,128)S(1)}, f32[1,8,128]{2,1,0:T(8,128)S(1)}, u32[]{:S(2)}, u32[]{:S(2)}) collective-permute-start(f32[1,8,128]{2,1,0:T(8,128)S(1)} %shard_map.58.refs_0_), channel_id=1, source_target_pairs={{0,8},{8,0},{16,24},{24,16},{1,9},{9,1},{17,25},{25,17},{2,10},{10... | collective-permute-start | bytes 12296 | tf_op jit(solution)/shard_map/ppermute | solution.py:246
  9.7 2.6 %collective-permute-start.7 = (f32[2,1,8,128]{3,2,1,0:T(8,128)S(1)}, f32[2,1,8,128]{3,2,1,0:T(8,128)S(1)}, u32[]{:S(2)}, u32[]{:S(2)}) collective-permute-start(f32[2,1,8,128]{3,2,1,0:T(8,128)S(1)} %get-tuple-element.86.pair), channel_id=1, source_target_pairs={{0,16},{8,24},{16,0},{24,8},{1,17},{9,25},{17,1},{25,9},{2,18},{10... | collective-permute-start | bytes 24584 | tf_op jit(solution)/shard_map/ppermute | solution.py:243
  12.3 2.6 %collective-permute-start = (bf16[1,128,4,128]{3,2,1,0:T(4,128)(2,1)S(1)}, bf16[1,128,4,128]{3,2,1,0:T(4,128)(2,1)S(1)}, u32[]{:S(2)}, u32[]{:S(2)}) collective-permute-start(bf16[1,128,4,128]{3,2,1,0:T(4,128)(2,1)S(1)} %get-tuple-element.55), channel_id=1, source_target_pairs={{0,8},{8,0},{16,24},{24,16},{1,9},{9,1},{17,25},{25,17},{2,10},{10... | collective-permute-start | bytes 393224 | tf_op jit(solution)/shard_map/cond/branch_1_fun/ppermute | solution.py:246
  15.3 0.7 %copy-start = (bf16[1,128,4,128]{3,2,1,0:T(4,128)(2,1)}, bf16[1,128,4,128]{3,2,1,0:T(4,128)(2,1)S(1)}, u32[]{:S(2)}) copy-start(bf16[1,128,4,128]{3,2,1,0:T(4,128)(2,1)S(1)} %get-tuple-element.113) | copy-start | bytes 393220

commit v4 on v3

v4 whole, which is shorter than its diff:
```python
import functools
import math

import jax
import jax.numpy as jnp
from jax import lax
from jax.experimental import pallas as pl
from jax.experimental.pallas import tpu as pltpu
from jax.sharding import PartitionSpec as P

QK = 64
SEGMENT = 64
CORES = 2
EXP_SCALE = math.log2(math.e) * QK ** (-0.5)
SPARE_BYTES = 2 << 20
PACK = 16
PARTS = 3
NT = (((1,), (1,)), ((), ()))


def each_head(heads, body):
    if heads <= 8:
        for head in range(heads):
            body(head)
    else:
        lax.fori_loop(0, heads, lambda head, c: (body(head), c)[1], 0)


def sources(peers):
    here = lax.axis_index("sp")
    cores = CORES if peers % CORES == 0 else 1
    chips = peers // cores
    chip, core = here // cores, here % cores
    straight = [lax.rem(chip + chips - r, chips) * cores + core for r in range(chips)]
    crossed = [lax.rem(chip + chips - r, chips) * cores + cores - 1 - core for r in range(chips)]
    if cores == 1:
        return here, [here], straight[1:], []
    return here, [here, crossed[0]], straight[1:], crossed[1:]


def widen(refs, wide):
    for i, ref in enumerate(refs):
        wide[i] = ref[...].astype(jnp.float32)
    return [wide.at[i] for i in range(len(refs))]


def split_rows(ref, head, heads, tokens):
    return ref[pl.ds(head, tokens, stride=heads), :].astype(jnp.bfloat16)


def head_rows(ref, head, tokens):
    return ref[pl.ds(head * tokens, tokens), :]


def hide(scores, here, source, tokens):
    queries = here * tokens + lax.rem(lax.broadcasted_iota(jnp.int32, scores.shape, 0), tokens)
    keys = source * tokens + lax.broadcasted_iota(jnp.int32, scores.shape, 1)
    return jnp.where(keys // SEGMENT <= queries // SEGMENT, scores, -jnp.inf)


def weigh(stacked, keys, srcs, here, tokens, floor):
    scores = [
        hide(lax.dot_general(stacked, key, NT, preferred_element_type=jnp.float32), here, source, tokens)
        for key, source in zip(keys, srcs)
    ]
    top = jnp.max(functools.reduce(jnp.maximum, scores), axis=1, keepdims=True)
    top = jnp.broadcast_to(top, scores[0].shape)
    if floor is not None:
        top = jnp.maximum(top, floor)
    raised = [jnp.exp2((block - top) * EXP_SCALE) for block in scores]
    total = jnp.sum(functools.reduce(jnp.add, raised), axis=1, keepdims=True)
    return top, raised, jnp.broadcast_to(total, scores[0].shape)


def weighted(blocks, values):
    return functools.reduce(
        jnp.add, [jnp.dot(block, value, preferred_element_type=jnp.float32) for block, value in zip(blocks, values)]
    )


def prepare(heads, tokens, query, key, value, gain, stacked, key_heads, value_heads, gain_tile, wide):
    query_wide, key_wide, value_wide = widen((query, key, value), wide)

    def body(head):
        rows = split_rows(query_wide, head, heads, tokens)
        first = lax.broadcasted_iota(jnp.int32, rows.shape, 1) < QK
        zero = jnp.zeros_like(rows)
        stacked[head] = jnp.concatenate([jnp.where(first, rows, zero), jnp.where(first, zero, rows)], axis=0)
        key_heads[pl.ds(head * tokens, tokens), :] = split_rows(key_wide, head, heads, tokens)
        value_heads[pl.ds(head * tokens, tokens), :] = split_rows(value_wide, head, heads, tokens)

    each_head(heads, body)
    gain_tile[...] = jnp.broadcast_to(gain[...], gain_tile.shape)


def pack(heads, tokens, key, value, key_pack, value_pack, wide):
    key_wide, value_wide = widen((key, value), wide)

    def body(head):
        key_pack[pl.ds(head * tokens, tokens), :] = split_rows(key_wide, head, heads, tokens)
        value_pack[pl.ds(head * tokens, tokens), :] = split_rows(value_wide, head, heads, tokens)

    each_head(heads, body)


def blank(key_pack, value_pack):
    for ref in (key_pack, value_pack):
        ref[...] = jnp.zeros_like(ref)


def stamp(rows, map_weight, value_in, value_pack, tile):
    value_pack[pl.ds(0, rows), :] = value_in[pl.ds(0, rows), :]
    for own in range(tile.shape[0]):
        rest = jnp.full((PACK, value_pack.shape[1]), map_weight[own])
        tile[own] = rest[: tile.shape[1]]
        row = lax.broadcasted_iota(jnp.int32, rest.shape, 0)
        packed = jnp.zeros_like(rest)
        for part in range(PARTS):
            piece = rest.astype(jnp.bfloat16).astype(jnp.float32)
            packed = jnp.where(row == part, piece, packed)
            rest = rest - piece
        value_pack[pl.ds(rows + own * PACK, PACK), :] = packed.astype(jnp.bfloat16)


def stamped(value_pack, rows, per_peer):
    found = []
    for own in range(per_peer):
        parts = value_pack[pl.ds(rows + own * PACK, PACK), :].astype(jnp.float32)
        found.append(sum(parts[i : i + 1] for i in range(PARTS)))
    return found


def near_scores(peers, heads, tokens, stacked, key_heads, gain, *refs):
    here, near, _, _ = sources(peers)
    tiles, keys = refs[: len(near)], refs[len(near) : -5]
    raised, level, gain_out, pair, wide = refs[-5:]
    keys_wide = widen(keys, wide)
    gain_out[...] = gain[...]
    for i, tile in enumerate(tiles):
        pair[i] = tile[...]

    def body(head):
        blocks = [head_rows(key_heads, head, tokens)] + [split_rows(ref, head, heads, tokens) for ref in keys_wide]
        peak, blocks, mass = weigh(stacked[head], blocks, near, here, tokens, None)
        inverse = 1.0 / mass
        level[head] = peak + jnp.log(mass) * QK**0.5
        for i, block in enumerate(blocks):
            raised[i, head] = (block * inverse).astype(jnp.bfloat16)

    each_head(heads, body)


def straight_scores(peers, heads, tokens, counts, stacked, near_raised, near_level, gain, pair, value_heads, *refs):
    here, _, straight, _ = sources(peers)
    n_side, n_near = counts
    values, keys = refs[:n_side], refs[n_side:-6]
    raised, level, summed, gain_out, pair_out, value_wide = refs[-6:]
    gain_out[...] = gain[...]
    pair_out[...] = pair[...]
    values_wide = widen(values, value_wide)

    def body(head):
        blocks = [head_rows(ref, head, tokens) for ref in keys]
        peak, blocks, mass = weigh(stacked[head], blocks, straight, here, tokens, near_level[head])
        prior = jnp.exp2((near_level[head] - peak) * EXP_SCALE)
        mass = prior + mass
        inverse = 1.0 / mass
        level[head] = peak + jnp.log(mass) * QK**0.5
        for i, block in enumerate(blocks):
            raised[i, head] = (block * inverse).astype(jnp.bfloat16)
        near_values = [head_rows(value_heads, head, tokens)] + [split_rows(v, head, heads, tokens) for v in values_wide]
        summed[head] = weighted([near_raised[i, head] for i in range(n_near)], near_values) * (prior * inverse)

    each_head(heads, body)


def owned(head, per_peer, here, held):
    second = jnp.zeros_like(held[0][0][0])
    for rows, source, by in held:
        for own in range(per_peer):
            here_too = source * per_peer + own == head
            if by is not None:
                here_too = jnp.logical_and(here_too, (source < here) if by == "pack" else (source > here))
            second += jnp.where(here_too, rows[own], 0.0)
    return second


def tile_rows(tiles, i, per_peer):
    return [tiles[i, own, 0:1, :] for own in range(per_peer)]


def by_pair(pairs, side, per_peer):
    straight, crossed = side
    found = [(tile_rows(pair, 0, per_peer), source, "pair") for pair, source in zip(pairs, straight)]
    return found + [(tile_rows(pair, 1, per_peer), source, "pair") for pair, source in zip(pairs, crossed)]


def last_scores(peers, heads, tokens, stacked, summed, level, far_raised, *refs):
    here, _, straight, crossed = sources(peers)
    values, keys, (weights, partial) = refs[: len(straight)], refs[len(straight) : -2], refs[-2:]

    def body(head):
        blocks = [head_rows(ref, head, tokens) for ref in keys]
        peak, blocks, mass = weigh(stacked[head], blocks, crossed, here, tokens, level[head])
        prior = jnp.exp2((level[head] - peak) * EXP_SCALE)
        inverse = 1.0 / (prior + mass)
        for i, block in enumerate(blocks):
            weights[i, head] = (block * inverse).astype(jnp.bfloat16)
        far_values = [head_rows(ref, head, tokens) for ref in values]
        far = weighted([far_raised[i, head] for i in range(len(straight))], far_values)
        partial[head] = (summed[head] + far) * (prior * inverse)

    each_head(heads, body)


def write_rows(attended, head, heads, tokens, gain, out_wide):
    mean_square = jnp.mean(attended * attended, axis=1, keepdims=True)
    out_wide[pl.ds(head, tokens, stride=heads), :] = attended * lax.rsqrt(mean_square + 1e-06) * gain[0:1, :]


def finish_near(peers, heads, tokens, summed, gain, near_pair, *refs):
    pairs, (out, out_wide) = refs[:-2], refs[-2:]
    here, near, *far = sources(peers)
    per_peer = heads // peers
    held = [(tile_rows(near_pair, i, per_peer), source, None) for i, source in enumerate(near)]
    held += by_pair(pairs, far, per_peer)

    def body(head):
        both = summed[head]
        attended = both[:tokens] - owned(head, per_peer, here, held) * both[tokens:]
        write_rows(attended, head, heads, tokens, gain, out_wide)

    each_head(heads, body)
    out[...] = out_wide[...].astype(out.dtype)


def finish(peers, heads, tokens, weights, partial, gain, near_pair, *refs):
    here, near, straight, crossed = sources(peers)
    ends = len(straight), len(straight) + len(crossed)
    far, last, pairs, (out, out_wide) = refs[: ends[0]], refs[ends[0] : ends[1]], refs[ends[1] : -2], refs[-2:]
    per_peer = heads // peers
    held = [(tile_rows(near_pair, i, per_peer), source, None) for i, source in enumerate(near)]
    for refs_in, side in ((far, straight), (last, crossed)):
        held += [(stamped(ref, heads * tokens, per_peer), source, "pack") for ref, source in zip(refs_in, side)]
    held += by_pair(pairs, (straight, crossed), per_peer) if pairs else []

    def body(head):
        both = partial[head] + weighted(
            [weights[i, head] for i in range(len(last))], [head_rows(ref, head, tokens) for ref in last]
        )
        attended = both[:tokens] - owned(head, per_peer, here, held) * both[tokens:]
        write_rows(attended, head, heads, tokens, gain, out_wide)

    each_head(heads, body)
    out[...] = out_wide[...].astype(out.dtype)


def hold(*refs):
    pass


def kernel(body, outs, scratch, fetched=False, keep=False, aliases=None):
    space = pl.BlockSpec(memory_space=pltpu.VMEM)
    held = sum(4 * math.prod(s.shape) for s in scratch if s.dtype == jnp.float32)
    held += sum(math.prod(o.shape) * o.dtype.itemsize for o in jax.tree.leaves(outs))

    def call(*args):
        limit = SPARE_BYTES + held + sum(a.size * a.dtype.itemsize for a in args)
        if fetched or keep:
            args = [pltpu.with_memory_space_constraint(a, pltpu.HBM if fetched else pltpu.VMEM) for a in args]
        return pl.pallas_call(
            body,
            out_shape=outs,
            in_specs=[pl.BlockSpec(memory_space=pltpu.SMEM) if a.ndim == 1 else space for a in args],
            out_specs=jax.tree.map(lambda _: space, outs),
            scratch_shapes=scratch,
            input_output_aliases={i: i for i in range(len(args))} if keep else aliases or {},
            compiler_params=pltpu.CompilerParams(vmem_limit_bytes=limit),
        )(*args)

    return call


def on_device(query_rows, key_rows, value_rows, map_weight, head_gain):
    peers = lax.axis_size("sp")
    _, tokens, heads, width = query_rows.shape
    cores = CORES if peers % CORES == 0 else 1
    chips = peers // cores
    rows = tokens * heads

    def turn(x, by):
        return lax.ppermute(x, "sp", [(i, (i + by * cores) % peers) for i in range(peers)])

    def swap(x):
        return lax.ppermute(x, "sp", [(i, i // cores * cores + cores - 1 - i % cores) for i in range(peers)])

    def flat(x):
        return x.reshape(rows, width)

    f32 = lambda *s: jax.ShapeDtypeStruct(s, jnp.float32)
    bf16 = lambda *s: jax.ShapeDtypeStruct(s, jnp.bfloat16)
    wide = lambda n: pltpu.VMEM((n, rows, width), jnp.float32)
    both = (heads, 2 * tokens, tokens)
    shift = range(1, chips)
    n_near, n_far, n_last = cores, chips - 1, (chips - 1) * (cores - 1)

    chip = lax.axis_index("sp") // cores
    packs = (bf16(rows, width), bf16(rows + heads // peers * PACK, width))

    def sender():
        return kernel(functools.partial(pack, heads, tokens), packs, [wide(2)])(flat(key_rows), flat(value_rows))

    def receiver():
        return kernel(blank, packs, [])()

    key_pack, value_pack = lax.cond(chip < chips - 1, sender, receiver)
    key_far = [turn(key_pack, r) for r in shift]
    value_pack, tile = kernel(
        functools.partial(stamp, rows), (packs[1], f32(heads // peers, 8, width)), [], aliases={1: 0}
    )(map_weight, value_pack)
    value_far = [turn(value_pack, r) for r in shift]
    tiles = [tile] + ([swap(tile)] if cores > 1 else [])
    key_near = [swap(key_rows)] if cores > 1 else []
    value_near = [swap(value_rows)] if cores > 1 else []
    stacked, key_heads, value_heads, gain_tile = kernel(
        functools.partial(prepare, heads, tokens),
        (bf16(heads, 2 * tokens, width), bf16(rows, width), bf16(rows, width), f32(8, width)),
        [wide(3)],
        fetched=True,
    )(flat(query_rows), flat(key_rows), flat(value_rows), head_gain.reshape(1, -1))
    near_raised, near_level, gain_tile, pair = kernel(
        functools.partial(near_scores, peers, heads, tokens),
        (bf16(n_near, *both), f32(*both), f32(8, width), f32(n_near, heads // peers, 8, width)),
        [wide(max(cores - 1, 1))],
    )(stacked, key_heads, gain_tile, *tiles, *map(flat, key_near))
    pairs = [turn(pair, r) for r in shift]
    key_last = [swap(x) for x in key_far] if cores > 1 else []
    far_raised, level, summed, gain_tile, pair_tile = kernel(
        functools.partial(straight_scores, peers, heads, tokens, (cores - 1, n_near)),
        (
            bf16(n_far, *both), f32(*both), f32(heads, 2 * tokens, width), f32(8, width), f32(*pair.shape),
        ),
        [wide(max(cores - 1, 1))],
    )(stacked, near_raised, near_level, gain_tile, pair, value_heads, *map(flat, value_near), *key_far)

    def stay(*arrays):
        return kernel(hold, tuple(jax.ShapeDtypeStruct(x.shape, x.dtype) for x in arrays), [], keep=True)(*arrays)

    middle = chips > 2
    arrived = stay(*value_far, *key_last, *(pairs if middle else ()))
    value_far, key_last, late = arrived[:n_far], arrived[n_far : n_far + n_last], arrived[n_far + n_last :]

    def later_chip():
        value_last = [swap(x) for x in value_far] if cores > 1 else []
        weights, partial = kernel(
            functools.partial(last_scores, peers, heads, tokens),
            (bf16(n_last, *both), f32(heads, 2 * tokens, width)),
            [],
        )(stacked, summed, level, far_raised, *value_far, *key_last)
        return kernel(
            functools.partial(finish, peers, heads, tokens),
            bf16(rows, width),
            [pltpu.VMEM((rows, width), jnp.float32)],
        )(weights, partial, gain_tile, pair_tile, *value_far, *value_last, *late)

    def no_rows():
        return kernel(hold, bf16(rows, width), [])()

    mixed = lax.cond(chip > 0, later_chip, no_rows)
    mixed, *pairs = stay(mixed, *pairs)

    def first_chip():
        return kernel(
            functools.partial(finish_near, peers, heads, tokens),
            bf16(rows, width),
            [pltpu.VMEM((rows, width), jnp.float32)],
        )(summed, gain_tile, pair_tile, *pairs)

    mixed = lax.cond(chip > 0, lambda: mixed, first_chip)
    return mixed.reshape(query_rows.shape)


def solution(mesh):
    rows = P("dp", "sp", None, None)

    return jax.shard_map(
        on_device,
        mesh=mesh,
        in_specs=(rows, rows, rows, P("sp"), P()),
        out_specs=rows,
        check_vma=False,
    )
```

time: 16.1 us -> 14.4 us (0.89)
  the two profiles are of different devices: /device:TPU:5 before, /device:TPU:0 now
where the time goes in v4:
time: 14.4 us; the launch traced here: 14.3 us
  starting transfers between devices  5.72 us (40%)
  Pallas kernels  3.64 us (25%)
  waiting for transfers between devices  3.47 us (24%)
  between operations  0.75 us (5%)
  local copies, waits for them, and re-layouts  0.66 us (5%)
    ppermute x3, starting transfers between devices, turn(): lax.ppermute(x, 'sp', [(i, (i + by * cores) % peers) for i in range(peers)])  4.84 us
    pallas_call x9, Pallas kernels, call(): pl.pallas_call(body, out_shape=outs, in_specs=[pl.BlockSpec(memory_space=...  3.64 us
    ppermute x3, waiting for transfers between devices, turn(): lax.ppermute(x, 'sp', [(i, (i + by * cores) % peers) for i in range(peers)])  3.46 us
    ppermute x4, starting transfers between devices, swap(): lax.ppermute(x, 'sp', [(i, i // cores * cores + cores - 1 - i % cores) fo...  0.88 us
    unnamed x3, local copies, waits for them, and re-layouts  0.66 us
  transfers between devices with their start and end apart: 7, of which 2 were waited for; matrix products, arithmetic and copies ran while one was open for 0% of the time, Pallas kernels for 17%

profile of v4, /device:TPU:0, one launch (start us, length us, event | category | flops | bytes accessed | tf_op | source)
XLA Modules:
  0.0 14.3 jit_solution(9340991895394974892)
XLA Ops:
  0.0 1.0 %conditional.3 = ((bf16[512,128]{1,0:T(8,128)(2,1)S(1)}, bf16[528,128]{1,0:T(8,128)(2,1)S(1)})) conditional(s32[]{:T(128)} %convert_element_type.8, () %tuple.25, (bf16[1,128,4,128]{3,2,1,0:T(4,128)(2,1)}, bf16[1,128,4,128]{3,2,1,0:T(4,128)(2,1)}) %tuple.26), branch_computations={%region_0.1_spmd, %region_1.2_spmd} | conditional | bytes 8 | solution.py:316
  0.0 1.0 %branch_1_fun.3 = (bf16[512,128]{1,0:T(8,128)(2,1)S(1)}, bf16[528,128]{1,0:T(8,128)(2,1)S(1)}) custom-call(bf16[512,128]{1,0:T(8,128)(2,1)} %bitcast.15, bf16[512,128]{1,0:T(8,128)(2,1)} %bitcast.17), custom_call_target="tpu_custom_call" | custom-call | tf_op jit(solution)/shard_map/cond/branch_1_fun/pallas_call | solution.py:271
  1.0 0.0 copy-start
  1.0 2.1 %collective-permute-start.4 = (bf16[512,128]{1,0:T(8,128)(2,1)S(1)}, bf16[512,128]{1,0:T(8,128)(2,1)S(1)}, u32[]{:S(2)}, u32[]{:S(2)}) collective-permute-start(bf16[512,128]{1,0:T(8,128)(2,1)S(1)} %get-tuple-element.89), channel_id=1, source_target_pairs={{0,16},{8,24},{16,0},{24,8},{1,17},{9,25},{17,1},{25,9},{2,18},{10... | collective-permute-start | bytes 393224 | tf_op jit(solution)/shard_map/ppermute | solution.py:292
  3.1 0.0 collective-permute-start.2
  3.8 0.3 %collective-permute-start.5 = (bf16[528,128]{1,0:T(8,128)(2,1)S(1)}, bf16[528,128]{1,0:T(8,128)(2,1)S(1)}, u32[]{:S(2)}, u32[]{:S(2)}) collective-permute-start(bf16[528,128]{1,0:T(8,128)(2,1)S(1)} %get-tuple-element.95), channel_id=1, source_target_pairs={{0,16},{8,24},{16,0},{24,8},{1,17},{9,25},{17,1},{25,9},{2,18},{10... | collective-permute-start | bytes 405512 | tf_op jit(solution)/shard_map/ppermute | solution.py:292
  4.1 0.0 copy-done
  4.1 0.4 %collective-permute-start.3 = (bf16[1,128,4,128]{3,2,1,0:T(4,128)(2,1)S(1)}, bf16[1,128,4,128]{3,2,1,0:T(4,128)(2,1)S(1)}, u32[]{:S(2)}, u32[]{:S(2)}) collective-permute-start(bf16[1,128,4,128]{3,2,1,0:T(4,128)(2,1)S(1)} %copy-done), channel_id=1, source_target_pairs={{0,8},{8,0},{16,24},{24,16},{1,9},{9,1},{17,25},{25,17},{2,10},{10... | collective-permute-start | bytes 393224 | tf_op jit(solution)/shard_map/ppermute | solution.py:295
  4.5 2.5 %collective-permute-done.4.refs_1_ = bf16[512,128]{1,0:T(8,128)(2,1)S(1)} collective-permute-done((bf16[512,128]{1,0:T(8,128)(2,1)S(1)}, bf16[512,128]{1,0:T(8,128)(2,1)S(1)}, u32[]{:S(2)}, u32[]{:S(2)}) %collective-permute-start.4) | collective-permute-done | bytes 131104 | tf_op jit(solution)/shard_map/ppermute | solution.py:292
  7.0 0.0 collective-permute-start.6
  7.0 0.5 %collective-permute-start.1 = (f32[1,8,128]{2,1,0:T(8,128)S(1)}, f32[1,8,128]{2,1,0:T(8,128)S(1)}, u32[]{:S(2)}, u32[]{:S(2)}) collective-permute-start(f32[1,8,128]{2,1,0:T(8,128)S(1)} %get-tuple-element.83.refs_0_), channel_id=1, source_target_pairs={{0,8},{8,0},{16,24},{24,16},{1,9},{9,1},{17,25},{25,17},{2,10},{10... | collective-permute-start | bytes 12296 | tf_op jit(solution)/shard_map/ppermute | solution.py:295
  7.5 1.1 %shard_map.57 = (bf16[4,256,128]{2,1,0:T(8,128)(2,1)S(1)}, bf16[512,128]{1,0:T(8,128)(2,1)S(1)}, bf16[512,128]{1,0:T(8,128)(2,1)S(1)}, f32[8,128]{1,0:T(8,128)S(1)}) custom-call(bf16[512,128]{1,0:T(8,128)(2,1)} %bitcast.18, bf16[512,128]{1,0:T(8,128)(2,1)} %bitcast.14, bf16[512,128]{1,0:T(8,128)(2,1)} %bitcast.16, f32[1,128]{1,0:T(1,128)} %bitcast.19), custom_call_target="tpu_custom_call" | custom-call | tf_op jit(solution)/shard_map/pallas_call | solution.py:271
  8.7 0.0 collective-permute-done.1.refs_1_
  8.7 0.0 collective-permute-done.2
  8.7 0.6 %shard_map.59 = (bf16[2,4,256,128]{3,2,1,0:T(8,128)(2,1)S(1)}, f32[4,256,128]{2,1,0:T(8,128)S(1)}, f32[8,128]{1,0:T(8,128)S(1)}, f32[2,1,8,128]{3,2,1,0:T(8,128)S(1)}) custom-call(bf16[4,256,128]{2,1,0:T(8,128)(2,1)S(1)} %get-tuple-element.79.stacked, bf16[512,128]{1,0:T(8,128)(2,1)S(1)} %get-tuple-element.80.key_heads, ...), custom_call_target="tpu_custom_call" | custom-call | tf_op jit(solution)/shard_map/pallas_call | solution.py:271
  9.3 2.5 %collective-permute-start.7 = (f32[2,1,8,128]{3,2,1,0:T(8,128)S(1)}, f32[2,1,8,128]{3,2,1,0:T(8,128)S(1)}, u32[]{:S(2)}, u32[]{:S(2)}) collective-permute-start(f32[2,1,8,128]{3,2,1,0:T(8,128)S(1)} %get-tuple-element.87.pair), channel_id=1, source_target_pairs={{0,16},{8,24},{16,0},{24,8},{1,17},{9,25},{17,1},{25,9},{2,18},{10... | collective-permute-start | bytes 24584 | tf_op jit(solution)/shard_map/ppermute | solution.py:292
  11.8 0.0 collective-permute-done.3
  11.8 0.6 %shard_map.60 = (bf16[1,4,256,128]{3,2,1,0:T(8,128)(2,1)S(1)}, f32[4,256,128]{2,1,0:T(8,128)S(1)}, f32[4,256,128]{2,1,0:T(8,128)S(1)}, f32[8,128]{1,0:T(8,128)S(1)}, f32[2,1,8,128]{3,2,1,0:T(8,128)S(1)}) custom-call(bf16[4,256,128]{2,1,0:T(8,128)(2,1)S(1)} %get-tuple-element.79.stacked, bf16[2,4,256,128]{3,2,1,0:T(8,128)(2,1)S(1)} %get-tuple-element.84.near_raised, ...), custom_call_target="tpu_custom_call" | custom-call | tf_op jit(solution)/shard_map/pallas_call | solution.py:271
  12.4 0.0 collective-permute-done.5.refs_0_
  12.4 0.0 collective-permute-done.6.refs_1_
  12.5 0.9 %collective-permute-done.7.refs_1_ = f32[2,1,8,128]{3,2,1,0:T(8,128)S(1)} collective-permute-done((f32[2,1,8,128]{3,2,1,0:T(8,128)S(1)}, f32[2,1,8,128]{3,2,1,0:T(8,128)S(1)}, u32[]{:S(2)}, u32[]{:S(2)}) %collective-permute-start.7) | collective-permute-done | bytes 8224 | tf_op jit(solution)/shard_map/ppermute | solution.py:292
  13.4 0.2 %conditional.5 = (bf16[1,128,4,128]{3,2,1,0:T(4,128)(2,1)S(1)}) conditional(s32[]{:T(128)} %convert_element_type.7, (f32[4,256,128]{2,1,0:T(8,128)S(1)}, f32[8,128]{1,0:T(8,128)S(1)}, f32[2,1,8,128]{3,2,1,0:T(8,128)S(1)}, f32[2,1,8,128]{3,2,1,0:T(8,128)S(1)}) %tuple.29, bf16[512,128]{1,0:T(8,128)(2,1)S(1)} %get-tuple-element.99), branch_computations={%region_4.5_spmd, %region_5.6_spmd} | conditional | bytes 8 | solution.py:379
  13.4 0.2 %branch_0_fun.5 = bf16[512,128]{1,0:T(8,128)(2,1)S(1)} custom-call(f32[4,256,128]{2,1,0:T(8,128)S(1)} %get-tuple-element.54.summed, f32[8,128]{1,0:T(8,128)S(1)} %get-tuple-element.55.gain, f32[2,1,8,128]{3,2,1,0:T(8,128)S(1)} %get-tuple-element.56.near_pair, f32[2,1,8,128]{3,2,1,0:T(8,128)S(1)} %get-tuple-element.57.refs_0_), custom_call_target="tpu_custom_call" | custom-call | tf_op jit(solution)/shard_map/cond/branch_0_fun/pallas_call | solution.py:271
  13.6 0.7 %copy.27 = bf16[1,128,4,128]{3,2,1,0:T(4,128)(2,1)} copy(bf16[1,128,4,128]{3,2,1,0:T(4,128)(2,1)S(1)} %get-tuple-element.100) | data formatting | bytes 262144
  (5 shorter events, 0.1 us)
Async XLA Ops:
  1.0 3.1 %copy-start = (bf16[1,128,4,128]{3,2,1,0:T(4,128)(2,1)S(1)}, bf16[1,128,4,128]{3,2,1,0:T(4,128)(2,1)}, u32[]{:S(2)}) copy-start(bf16[1,128,4,128]{3,2,1,0:T(4,128)(2,1)} %param.13) | copy-start | bytes 393220
  1.0 6.0 %collective-permute-start.4 = (bf16[512,128]{1,0:T(8,128)(2,1)S(1)}, bf16[512,128]{1,0:T(8,128)(2,1)S(1)}, u32[]{:S(2)}, u32[]{:S(2)}) collective-permute-start(bf16[512,128]{1,0:T(8,128)(2,1)S(1)} %get-tuple-element.89), channel_id=1, source_target_pairs={{0,16},{8,24},{16,0},{24,8},{1,17},{9,25},{17,1},{25,9},{2,18},{10... | collective-permute-start | bytes 393224 | tf_op jit(solution)/shard_map/ppermute | solution.py:292
  3.1 5.6 %collective-permute-start.2 = (bf16[1,128,4,128]{3,2,1,0:T(4,128)(2,1)}, bf16[1,128,4,128]{3,2,1,0:T(4,128)(2,1)S(1)}, u32[]{:S(2)}, u32[]{:S(2)}) collective-permute-start(bf16[1,128,4,128]{3,2,1,0:T(4,128)(2,1)} %param.12), channel_id=1, source_target_pairs={{0,8},{8,0},{16,24},{24,16},{1,9},{9,1},{17,25},{25,17},{2,10},{10... | collective-permute-start | bytes 393224 | tf_op jit(solution)/shard_map/ppermute | solution.py:295
  3.8 8.6 %collective-permute-start.5 = (bf16[528,128]{1,0:T(8,128)(2,1)S(1)}, bf16[528,128]{1,0:T(8,128)(2,1)S(1)}, u32[]{:S(2)}, u32[]{:S(2)}) collective-permute-start(bf16[528,128]{1,0:T(8,128)(2,1)S(1)} %get-tuple-element.95), channel_id=1, source_target_pairs={{0,16},{8,24},{16,0},{24,8},{1,17},{9,25},{17,1},{25,9},{2,18},{10... | collective-permute-start | bytes 405512 | tf_op jit(solution)/shard_map/ppermute | solution.py:292
  4.1 7.7 %collective-permute-start.3 = (bf16[1,128,4,128]{3,2,1,0:T(4,128)(2,1)S(1)}, bf16[1,128,4,128]{3,2,1,0:T(4,128)(2,1)S(1)}, u32[]{:S(2)}, u32[]{:S(2)}) collective-permute-start(bf16[1,128,4,128]{3,2,1,0:T(4,128)(2,1)S(1)} %copy-done), channel_id=1, source_target_pairs={{0,8},{8,0},{16,24},{24,16},{1,9},{9,1},{17,25},{25,17},{2,10},{10... | collective-permute-start | bytes 393224 | tf_op jit(solution)/shard_map/ppermute | solution.py:295
  7.0 5.4 %collective-permute-start.6 = (bf16[512,128]{1,0:T(8,128)(2,1)S(1)}, bf16[512,128]{1,0:T(8,128)(2,1)S(1)}, u32[]{:S(2)}, u32[]{:S(2)}) collective-permute-start(bf16[512,128]{1,0:T(8,128)(2,1)S(1)} %collective-permute-done.4.refs_1_), channel_id=1, source_target_pairs={{0,8},{8,0},{16,24},{24,16},{1,9},{9,1},{17,25},{25,17},{2,10},{10... | collective-permute-start | bytes 393224 | tf_op jit(solution)/shard_map/ppermute | solution.py:295
  7.0 1.7 %collective-permute-start.1 = (f32[1,8,128]{2,1,0:T(8,128)S(1)}, f32[1,8,128]{2,1,0:T(8,128)S(1)}, u32[]{:S(2)}, u32[]{:S(2)}) collective-permute-start(f32[1,8,128]{2,1,0:T(8,128)S(1)} %get-tuple-element.83.refs_0_), channel_id=1, source_target_pairs={{0,8},{8,0},{16,24},{24,16},{1,9},{9,1},{17,25},{25,17},{2,10},{10... | collective-permute-start | bytes 12296 | tf_op jit(solution)/shard_map/ppermute | solution.py:295
  9.3 4.1 %collective-permute-start.7 = (f32[2,1,8,128]{3,2,1,0:T(8,128)S(1)}, f32[2,1,8,128]{3,2,1,0:T(8,128)S(1)}, u32[]{:S(2)}, u32[]{:S(2)}) collective-permute-start(f32[2,1,8,128]{3,2,1,0:T(8,128)S(1)} %get-tuple-element.87.pair), channel_id=1, source_target_pairs={{0,16},{8,24},{16,0},{24,8},{1,17},{9,25},{17,1},{25,9},{2,18},{10... | collective-permute-start | bytes 24584 | tf_op jit(solution)/shard_map/ppermute | solution.py:292

commit v5 on v4

--- a/solution.py
+++ b/solution.py
@@ -195,11 +195,15 @@
     return found + [(tile_rows(pair, 1, per_peer), source, "pair") for pair, source in zip(pairs, crossed)]
 
 
-def last_scores(peers, heads, tokens, stacked, summed, level, far_raised, *refs):
-    here, _, straight, crossed = sources(peers)
-    values, keys, (weights, partial) = refs[: len(straight)], refs[len(straight) : -2], refs[-2:]
-
-    def body(head):
+def last_scores(peers, heads, tokens, stacked, summed, level, far_raised, near_pair, *refs):
+    here, near, straight, crossed = sources(peers)
+    values, keys, (weights, partial, second) = refs[: len(straight)], refs[len(straight) : -3], refs[-3:]
+    per_peer = heads // peers
+    held = [(tile_rows(near_pair, i, per_peer), source, None) for i, source in enumerate(near)]
+    held += [(stamped(ref, heads * tokens, per_peer), source, "pack") for ref, source in zip(values, straight)]
+
+    def body(head):
+        second[head] = jnp.broadcast_to(owned(head, per_peer, here, held), second.shape[1:])
         blocks = [head_rows(ref, head, tokens) for ref in keys]
         peak, blocks, mass = weigh(stacked[head], blocks, crossed, here, tokens, level[head])
         prior = jnp.exp2((level[head] - peak) * EXP_SCALE)
@@ -234,21 +238,21 @@
     out[...] = out_wide[...].astype(out.dtype)
 
 
-def finish(peers, heads, tokens, weights, partial, gain, near_pair, *refs):
-    here, near, straight, crossed = sources(peers)
-    ends = len(straight), len(straight) + len(crossed)
-    far, last, pairs, (out, out_wide) = refs[: ends[0]], refs[ends[0] : ends[1]], refs[ends[1] : -2], refs[-2:]
+def finish(peers, heads, tokens, weights, partial, known, gain, *refs):
+    here, _, straight, crossed = sources(peers)
+    last, pairs, (out, out_wide) = refs[: len(crossed)], refs[len(crossed) : -2], refs[-2:]
     per_peer = heads // peers
-    held = [(tile_rows(near_pair, i, per_peer), source, None) for i, source in enumerate(near)]
-    for refs_in, side in ((far, straight), (last, crossed)):
-        held += [(stamped(ref, heads * tokens, per_peer), source, "pack") for ref, source in zip(refs_in, side)]
+    held = [(stamped(ref, heads * tokens, per_peer), source, "pack") for ref, source in zip(last, crossed)]
     held += by_pair(pairs, (straight, crossed), per_peer) if pairs else []
 
     def body(head):
         both = partial[head] + weighted(
             [weights[i, head] for i in range(len(last))], [head_rows(ref, head, tokens) for ref in last]
         )
-        attended = both[:tokens] - owned(head, per_peer, here, held) * both[tokens:]
+        second = known[head, 0:1, :]
+        if held:
+            second += owned(head, per_peer, here, held)
+        attended = both[:tokens] - second * both[tokens:]
         write_rows(attended, head, heads, tokens, gain, out_wide)
 
     each_head(heads, body)
@@ -311,7 +315,7 @@
         return kernel(functools.partial(pack, heads, tokens), packs, [wide(2)])(flat(key_rows), flat(value_rows))
 
     def receiver():
-        return kernel(blank, packs, [])()
+        return kernel(blank if chips > 2 else hold, packs, [])()
 
     key_pack, value_pack = lax.cond(chip < chips - 1, sender, receiver)
     key_far = [turn(key_pack, r) for r in shift]
@@ -352,16 +356,16 @@
 
     def later_chip():
         value_last = [swap(x) for x in value_far] if cores > 1 else []
-        weights, partial = kernel(
+        weights, partial, known = kernel(
             functools.partial(last_scores, peers, heads, tokens),
-            (bf16(n_last, *both), f32(heads, 2 * tokens, width)),
+            (bf16(n_last, *both), f32(heads, 2 * tokens, width), f32(heads, 8, width)),
             [],
-        )(stacked, summed, level, far_raised, *value_far, *key_last)
+        )(stacked, summed, level, far_raised, pair_tile, *value_far, *key_last)
         return kernel(
             functools.partial(finish, peers, heads, tokens),
             bf16(rows, width),
             [pltpu.VMEM((rows, width), jnp.float32)],
-        )(weights, partial, gain_tile, pair_tile, *value_far, *value_last, *late)
+        )(weights, partial, known, gain_tile, *value_last, *late)
 
     def no_rows():
         return kernel(hold, bf16(rows, width), [])()

time: 14.4 us -> 14.3 us (level)
  starting transfers between devices: 5.72 us -> 5.36 us
  waiting for transfers between devices: 3.47 us -> 3.72 us
    ppermute x3, waiting for transfers between devices: 3.46 us -> 3.71 us  [turn(): lax.ppermute(x, 'sp', [(i, (i + by * cores) % peers) for i in range(peers)])]
    ppermute x3, starting transfers between devices: 4.84 us -> 4.6 us  [turn(): lax.ppermute(x, 'sp', [(i, (i + by * cores) % peers) for i in range(peers)])]
where the time goes in v5:
time: 14.3 us; the launch traced here: 14.2 us
  starting transfers between devices  5.36 us (37%)
  waiting for transfers between devices  3.72 us (26%)
  Pallas kernels  3.64 us (25%)
  between operations  0.75 us (5%)
  local copies, waits for them, and re-layouts  0.66 us (5%)
    ppermute x3, starting transfers between devices, turn(): lax.ppermute(x, 'sp', [(i, (i + by * cores) % peers) for i in range(peers)])  4.6 us
    ppermute x3, waiting for transfers between devices, turn(): lax.ppermute(x, 'sp', [(i, (i + by * cores) % peers) for i in range(peers)])  3.71 us
    pallas_call x9, Pallas kernels, call(): pl.pallas_call(body, out_shape=outs, in_specs=[pl.BlockSpec(memory_space=...  3.64 us
    ppermute x4, starting transfers between devices, swap(): lax.ppermute(x, 'sp', [(i, i // cores * cores + cores - 1 - i % cores) fo...  0.76 us
    unnamed x3, local copies, waits for them, and re-layouts  0.66 us
  transfers between devices with their start and end apart: 7, of which 2 were waited for; matrix products, arithmetic and copies ran while one was open for 0% of the time, Pallas kernels for 17%

profile of v5, /device:TPU:0, one launch (start us, length us, event | category | flops | bytes accessed | tf_op | source)
XLA Modules:
  0.0 14.2 jit_solution(649113810703187188)
XLA Ops:
  0.0 1.0 %conditional.3 = ((bf16[512,128]{1,0:T(8,128)(2,1)S(1)}, bf16[528,128]{1,0:T(8,128)(2,1)S(1)})) conditional(s32[]{:T(128)} %convert_element_type.8, () %tuple.25, (bf16[1,128,4,128]{3,2,1,0:T(4,128)(2,1)}, bf16[1,128,4,128]{3,2,1,0:T(4,128)(2,1)}) %tuple.26), branch_computations={%region_0.1_spmd, %region_1.2_spmd} | conditional | bytes 8 | solution.py:320
  0.0 1.0 %branch_1_fun.3 = (bf16[512,128]{1,0:T(8,128)(2,1)S(1)}, bf16[528,128]{1,0:T(8,128)(2,1)S(1)}) custom-call(bf16[512,128]{1,0:T(8,128)(2,1)} %bitcast.15, bf16[512,128]{1,0:T(8,128)(2,1)} %bitcast.17), custom_call_target="tpu_custom_call" | custom-call | tf_op jit(solution)/shard_map/cond/branch_1_fun/pallas_call | solution.py:275
  1.0 0.0 copy-start
  1.0 2.0 %collective-permute-start.4 = (bf16[512,128]{1,0:T(8,128)(2,1)S(1)}, bf16[512,128]{1,0:T(8,128)(2,1)S(1)}, u32[]{:S(2)}, u32[]{:S(2)}) collective-permute-start(bf16[512,128]{1,0:T(8,128)(2,1)S(1)} %get-tuple-element.90), channel_id=1, source_target_pairs={{0,16},{8,24},{16,0},{24,8},{1,17},{9,25},{17,1},{25,9},{2,18},{10... | collective-permute-start | bytes 393224 | tf_op jit(solution)/shard_map/ppermute | solution.py:296
  3.0 0.0 collective-permute-start.2
  3.7 0.4 %collective-permute-start.5 = (bf16[528,128]{1,0:T(8,128)(2,1)S(1)}, bf16[528,128]{1,0:T(8,128)(2,1)S(1)}, u32[]{:S(2)}, u32[]{:S(2)}) collective-permute-start(bf16[528,128]{1,0:T(8,128)(2,1)S(1)} %get-tuple-element.96), channel_id=1, source_target_pairs={{0,16},{8,24},{16,0},{24,8},{1,17},{9,25},{17,1},{25,9},{2,18},{10... | collective-permute-start | bytes 405512 | tf_op jit(solution)/shard_map/ppermute | solution.py:296
  4.1 0.0 copy-done
  4.1 0.2 %collective-permute-start.3 = (bf16[1,128,4,128]{3,2,1,0:T(4,128)(2,1)S(1)}, bf16[1,128,4,128]{3,2,1,0:T(4,128)(2,1)S(1)}, u32[]{:S(2)}, u32[]{:S(2)}) collective-permute-start(bf16[1,128,4,128]{3,2,1,0:T(4,128)(2,1)S(1)} %copy-done), channel_id=1, source_target_pairs={{0,8},{8,0},{16,24},{24,16},{1,9},{9,1},{17,25},{25,17},{2,10},{10... | collective-permute-start | bytes 393224 | tf_op jit(solution)/shard_map/ppermute | solution.py:299
  4.4 2.8 %collective-permute-done.4.refs_1_ = bf16[512,128]{1,0:T(8,128)(2,1)S(1)} collective-permute-done((bf16[512,128]{1,0:T(8,128)(2,1)S(1)}, bf16[512,128]{1,0:T(8,128)(2,1)S(1)}, u32[]{:S(2)}, u32[]{:S(2)}) %collective-permute-start.4) | collective-permute-done | bytes 131104 | tf_op jit(solution)/shard_map/ppermute | solution.py:296
  7.1 0.0 collective-permute-start.6
  7.1 0.5 %collective-permute-start.1 = (f32[1,8,128]{2,1,0:T(8,128)S(1)}, f32[1,8,128]{2,1,0:T(8,128)S(1)}, u32[]{:S(2)}, u32[]{:S(2)}) collective-permute-start(f32[1,8,128]{2,1,0:T(8,128)S(1)} %get-tuple-element.84.refs_0_), channel_id=1, source_target_pairs={{0,8},{8,0},{16,24},{24,16},{1,9},{9,1},{17,25},{25,17},{2,10},{10... | collective-permute-start | bytes 12296 | tf_op jit(solution)/shard_map/ppermute | solution.py:299
  7.7 1.1 %shard_map.57 = (bf16[4,256,128]{2,1,0:T(8,128)(2,1)S(1)}, bf16[512,128]{1,0:T(8,128)(2,1)S(1)}, bf16[512,128]{1,0:T(8,128)(2,1)S(1)}, f32[8,128]{1,0:T(8,128)S(1)}) custom-call(bf16[512,128]{1,0:T(8,128)(2,1)} %bitcast.18, bf16[512,128]{1,0:T(8,128)(2,1)} %bitcast.14, bf16[512,128]{1,0:T(8,128)(2,1)} %bitcast.16, f32[1,128]{1,0:T(1,128)} %bitcast.19), custom_call_target="tpu_custom_call" | custom-call | tf_op jit(solution)/shard_map/pallas_call | solution.py:275
  8.8 0.0 collective-permute-done.1.refs_1_
  8.8 0.0 collective-permute-done.2
  8.8 0.6 %shard_map.59 = (bf16[2,4,256,128]{3,2,1,0:T(8,128)(2,1)S(1)}, f32[4,256,128]{2,1,0:T(8,128)S(1)}, f32[8,128]{1,0:T(8,128)S(1)}, f32[2,1,8,128]{3,2,1,0:T(8,128)S(1)}) custom-call(bf16[4,256,128]{2,1,0:T(8,128)(2,1)S(1)} %get-tuple-element.80.stacked, bf16[512,128]{1,0:T(8,128)(2,1)S(1)} %get-tuple-element.81.key_heads, ...), custom_call_target="tpu_custom_call" | custom-call | tf_op jit(solution)/shard_map/pallas_call | solution.py:275
  9.4 2.2 %collective-permute-start.7 = (f32[2,1,8,128]{3,2,1,0:T(8,128)S(1)}, f32[2,1,8,128]{3,2,1,0:T(8,128)S(1)}, u32[]{:S(2)}, u32[]{:S(2)}) collective-permute-start(f32[2,1,8,128]{3,2,1,0:T(8,128)S(1)} %get-tuple-element.88.pair), channel_id=1, source_target_pairs={{0,16},{8,24},{16,0},{24,8},{1,17},{9,25},{17,1},{25,9},{2,18},{10... | collective-permute-start | bytes 24584 | tf_op jit(solution)/shard_map/ppermute | solution.py:296
  11.7 0.0 collective-permute-done.3
  11.7 0.6 %shard_map.60 = (bf16[1,4,256,128]{3,2,1,0:T(8,128)(2,1)S(1)}, f32[4,256,128]{2,1,0:T(8,128)S(1)}, f32[4,256,128]{2,1,0:T(8,128)S(1)}, f32[8,128]{1,0:T(8,128)S(1)}, f32[2,1,8,128]{3,2,1,0:T(8,128)S(1)}) custom-call(bf16[4,256,128]{2,1,0:T(8,128)(2,1)S(1)} %get-tuple-element.80.stacked, bf16[2,4,256,128]{3,2,1,0:T(8,128)(2,1)S(1)} %get-tuple-element.85.near_raised, ...), custom_call_target="tpu_custom_call" | custom-call | tf_op jit(solution)/shard_map/pallas_call | solution.py:275
  12.3 0.0 collective-permute-done.5.refs_0_
  12.3 0.0 collective-permute-done.6.refs_1_
  12.4 0.9 %collective-permute-done.7.refs_1_ = f32[2,1,8,128]{3,2,1,0:T(8,128)S(1)} collective-permute-done((f32[2,1,8,128]{3,2,1,0:T(8,128)S(1)}, f32[2,1,8,128]{3,2,1,0:T(8,128)S(1)}, u32[]{:S(2)}, u32[]{:S(2)}) %collective-permute-start.7) | collective-permute-done | bytes 8224 | tf_op jit(solution)/shard_map/ppermute | solution.py:296
  13.3 0.2 %conditional.5 = (bf16[1,128,4,128]{3,2,1,0:T(4,128)(2,1)S(1)}) conditional(s32[]{:T(128)} %convert_element_type.7, (f32[4,256,128]{2,1,0:T(8,128)S(1)}, f32[8,128]{1,0:T(8,128)S(1)}, f32[2,1,8,128]{3,2,1,0:T(8,128)S(1)}, f32[2,1,8,128]{3,2,1,0:T(8,128)S(1)}) %tuple.29, bf16[512,128]{1,0:T(8,128)(2,1)S(1)} %get-tuple-element.100), branch_computations={%region_4.5_spmd, %region_5.6_spmd} | conditional | bytes 8 | solution.py:383
  13.3 0.2 %branch_0_fun.5 = bf16[512,128]{1,0:T(8,128)(2,1)S(1)} custom-call(f32[4,256,128]{2,1,0:T(8,128)S(1)} %get-tuple-element.55.summed, f32[8,128]{1,0:T(8,128)S(1)} %get-tuple-element.56.gain, f32[2,1,8,128]{3,2,1,0:T(8,128)S(1)} %get-tuple-element.57.near_pair, f32[2,1,8,128]{3,2,1,0:T(8,128)S(1)} %get-tuple-element.58.refs_0_), custom_call_target="tpu_custom_call" | custom-call | tf_op jit(solution)/shard_map/cond/branch_0_fun/pallas_call | solution.py:275
  13.5 0.7 %copy.27 = bf16[1,128,4,128]{3,2,1,0:T(4,128)(2,1)} copy(bf16[1,128,4,128]{3,2,1,0:T(4,128)(2,1)S(1)} %get-tuple-element.101) | data formatting | bytes 262144
  (5 shorter events, 0.1 us)
Async XLA Ops:
  1.0 3.1 %copy-start = (bf16[1,128,4,128]{3,2,1,0:T(4,128)(2,1)S(1)}, bf16[1,128,4,128]{3,2,1,0:T(4,128)(2,1)}, u32[]{:S(2)}) copy-start(bf16[1,128,4,128]{3,2,1,0:T(4,128)(2,1)} %param.13) | copy-start | bytes 393220
  1.0 6.1 %collective-permute-start.4 = (bf16[512,128]{1,0:T(8,128)(2,1)S(1)}, bf16[512,128]{1,0:T(8,128)(2,1)S(1)}, u32[]{:S(2)}, u32[]{:S(2)}) collective-permute-start(bf16[512,128]{1,0:T(8,128)(2,1)S(1)} %get-tuple-element.90), channel_id=1, source_target_pairs={{0,16},{8,24},{16,0},{24,8},{1,17},{9,25},{17,1},{25,9},{2,18},{10... | collective-permute-start | bytes 393224 | tf_op jit(solution)/shard_map/ppermute | solution.py:296
  3.0 5.8 %collective-permute-start.2 = (bf16[1,128,4,128]{3,2,1,0:T(4,128)(2,1)}, bf16[1,128,4,128]{3,2,1,0:T(4,128)(2,1)S(1)}, u32[]{:S(2)}, u32[]{:S(2)}) collective-permute-start(bf16[1,128,4,128]{3,2,1,0:T(4,128)(2,1)} %param.12), channel_id=1, source_target_pairs={{0,8},{8,0},{16,24},{24,16},{1,9},{9,1},{17,25},{25,17},{2,10},{10... | collective-permute-start | bytes 393224 | tf_op jit(solution)/shard_map/ppermute | solution.py:299
  3.7 8.6 %collective-permute-start.5 = (bf16[528,128]{1,0:T(8,128)(2,1)S(1)}, bf16[528,128]{1,0:T(8,128)(2,1)S(1)}, u32[]{:S(2)}, u32[]{:S(2)}) collective-permute-start(bf16[528,128]{1,0:T(8,128)(2,1)S(1)} %get-tuple-element.96), channel_id=1, source_target_pairs={{0,16},{8,24},{16,0},{24,8},{1,17},{9,25},{17,1},{25,9},{2,18},{10... | collective-permute-start | bytes 405512 | tf_op jit(solution)/shard_map/ppermute | solution.py:296
  4.1 7.6 %collective-permute-start.3 = (bf16[1,128,4,128]{3,2,1,0:T(4,128)(2,1)S(1)}, bf16[1,128,4,128]{3,2,1,0:T(4,128)(2,1)S(1)}, u32[]{:S(2)}, u32[]{:S(2)}) collective-permute-start(bf16[1,128,4,128]{3,2,1,0:T(4,128)(2,1)S(1)} %copy-done), channel_id=1, source_target_pairs={{0,8},{8,0},{16,24},{24,16},{1,9},{9,1},{17,25},{25,17},{2,10},{10... | collective-permute-start | bytes 393224 | tf_op jit(solution)/shard_map/ppermute | solution.py:299
  7.1 5.2 %collective-permute-start.6 = (bf16[512,128]{1,0:T(8,128)(2,1)S(1)}, bf16[512,128]{1,0:T(8,128)(2,1)S(1)}, u32[]{:S(2)}, u32[]{:S(2)}) collective-permute-start(bf16[512,128]{1,0:T(8,128)(2,1)S(1)} %collective-permute-done.4.refs_1_), channel_id=1, source_target_pairs={{0,8},{8,0},{16,24},{24,16},{1,9},{9,1},{17,25},{25,17},{2,10},{10... | collective-permute-start | bytes 393224 | tf_op jit(solution)/shard_map/ppermute | solution.py:299
  7.1 1.7 %collective-permute-start.1 = (f32[1,8,128]{2,1,0:T(8,128)S(1)}, f32[1,8,128]{2,1,0:T(8,128)S(1)}, u32[]{:S(2)}, u32[]{:S(2)}) collective-permute-start(f32[1,8,128]{2,1,0:T(8,128)S(1)} %get-tuple-element.84.refs_0_), channel_id=1, source_target_pairs={{0,8},{8,0},{16,24},{24,16},{1,9},{9,1},{17,25},{25,17},{2,10},{10... | collective-permute-start | bytes 12296 | tf_op jit(solution)/shard_map/ppermute | solution.py:299
  9.4 3.9 %collective-permute-start.7 = (f32[2,1,8,128]{3,2,1,0:T(8,128)S(1)}, f32[2,1,8,128]{3,2,1,0:T(8,128)S(1)}, u32[]{:S(2)}, u32[]{:S(2)}) collective-permute-start(f32[2,1,8,128]{3,2,1,0:T(8,128)S(1)} %get-tuple-element.88.pair), channel_id=1, source_target_pairs={{0,16},{8,24},{16,0},{24,8},{1,17},{9,25},{17,1},{25,9},{2,18},{10... | collective-permute-start | bytes 24584 | tf_op jit(solution)/shard_map/ppermute | solution.py:296

commit v6 on v5

--- a/solution.py
+++ b/solution.py
@@ -15,6 +15,7 @@
 SPARE_BYTES = 2 << 20
 PACK = 16
 PARTS = 3
+PIECES = 1
 NT = (((1,), (1,)), ((), ()))
 
 
@@ -222,8 +223,20 @@
     out_wide[pl.ds(head, tokens, stride=heads), :] = attended * lax.rsqrt(mean_square + 1e-06) * gain[0:1, :]
 
 
+def write_out(out, out_wide, out_rows, sems):
+    step = out_rows.shape[0] // PIECES
+    moves = []
+    for i in range(PIECES):
+        piece = pl.ds(i * step, step)
+        out_rows[piece, :] = out_wide[piece, :].astype(out_rows.dtype)
+        moves.append(pltpu.make_async_copy(out_rows.at[piece], out.at[piece], sems.at[i]))
+        moves[-1].start()
+    for move in moves:
+        move.wait()
+
+
 def finish_near(peers, heads, tokens, summed, gain, near_pair, *refs):
-    pairs, (out, out_wide) = refs[:-2], refs[-2:]
+    pairs, (out, out_wide, out_rows, sems) = refs[:-4], refs[-4:]
     here, near, *far = sources(peers)
     per_peer = heads // peers
     held = [(tile_rows(near_pair, i, per_peer), source, None) for i, source in enumerate(near)]
@@ -235,12 +248,12 @@
         write_rows(attended, head, heads, tokens, gain, out_wide)
 
     each_head(heads, body)
-    out[...] = out_wide[...].astype(out.dtype)
+    write_out(out, out_wide, out_rows, sems)
 
 
 def finish(peers, heads, tokens, weights, partial, known, gain, *refs):
     here, _, straight, crossed = sources(peers)
-    last, pairs, (out, out_wide) = refs[: len(crossed)], refs[len(crossed) : -2], refs[-2:]
+    last, pairs, (out, out_wide, out_rows, sems) = refs[: len(crossed)], refs[len(crossed) : -4], refs[-4:]
     per_peer = heads // peers
     held = [(stamped(ref, heads * tokens, per_peer), source, "pack") for ref, source in zip(last, crossed)]
     held += by_pair(pairs, (straight, crossed), per_peer) if pairs else []
@@ -256,14 +269,14 @@
         write_rows(attended, head, heads, tokens, gain, out_wide)
 
     each_head(heads, body)
-    out[...] = out_wide[...].astype(out.dtype)
+    write_out(out, out_wide, out_rows, sems)
 
 
 def hold(*refs):
     pass
 
 
-def kernel(body, outs, scratch, fetched=False, keep=False, aliases=None):
+def kernel(body, outs, scratch, fetched=False, keep=False, aliases=None, away=False):
     space = pl.BlockSpec(memory_space=pltpu.VMEM)
     held = sum(4 * math.prod(s.shape) for s in scratch if s.dtype == jnp.float32)
     held += sum(math.prod(o.shape) * o.dtype.itemsize for o in jax.tree.leaves(outs))
@@ -274,9 +287,9 @@
             args = [pltpu.with_memory_space_constraint(a, pltpu.HBM if fetched else pltpu.VMEM) for a in args]
         return pl.pallas_call(
             body,
-            out_shape=outs,
+            out_shape=pltpu.HBM(outs.shape, outs.dtype) if away else outs,
             in_specs=[pl.BlockSpec(memory_space=pltpu.SMEM) if a.ndim == 1 else space for a in args],
-            out_specs=jax.tree.map(lambda _: space, outs),
+            out_specs=jax.tree.map(lambda _: pl.BlockSpec(memory_space=pltpu.HBM) if away else space, outs),
             scratch_shapes=scratch,
             input_output_aliases={i: i for i in range(len(args))} if keep else aliases or {},
             compiler_params=pltpu.CompilerParams(vmem_limit_bytes=limit),
@@ -351,6 +364,11 @@
         return kernel(hold, tuple(jax.ShapeDtypeStruct(x.shape, x.dtype) for x in arrays), [], keep=True)(*arrays)
 
     middle = chips > 2
+    writer = [
+        pltpu.VMEM((rows, width), jnp.float32),
+        pltpu.VMEM((rows, width), jnp.bfloat16),
+        pltpu.SemaphoreType.DMA((PIECES,)),
+    ]
     arrived = stay(*value_far, *key_last, *(pairs if middle else ()))
     value_far, key_last, late = arrived[:n_far], arrived[n_far : n_far + n_last], arrived[n_far + n_last :]
 
@@ -364,20 +382,23 @@
         return kernel(
             functools.partial(finish, peers, heads, tokens),
             bf16(rows, width),
-            [pltpu.VMEM((rows, width), jnp.float32)],
+            writer,
+            away=True,
         )(weights, partial, known, gain_tile, *value_last, *late)
 
     def no_rows():
-        return kernel(hold, bf16(rows, width), [])()
+        return kernel(hold, bf16(rows, width), [], away=True)()
 
     mixed = lax.cond(chip > 0, later_chip, no_rows)
-    mixed, *pairs = stay(mixed, *pairs)
+    mixed, pairs = lax.optimization_barrier((mixed, pairs))
+    pairs = stay(*pairs)
 
     def first_chip():
         return kernel(
             functools.partial(finish_near, peers, heads, tokens),
             bf16(rows, width),
-            [pltpu.VMEM((rows, width), jnp.float32)],
+            writer,
+            away=True,
         )(summed, gain_tile, pair_tile, *pairs)
 
     mixed = lax.cond(chip > 0, lambda: mixed, first_chip)

time: 14.3 us -> 14.3 us (level)
  Pallas kernels: 3.64 us -> 4.3 us
  local copies, waits for them, and re-layouts: 0.66 us -> 0.01 us
    pallas_call x9, Pallas kernels: 3.64 us -> 4.3 us  [call(): pl.pallas_call(body, out_shape=pltpu.HBM(outs.shape, outs.dtype) if away...]
    unnamed x3 -> x2, local copies, waits for them, and re-layouts: 0.66 us -> 0.01 us
where the time goes in v6:
time: 14.3 us; the launch traced here: 14.2 us
  starting transfers between devices  5.36 us (37%)
  Pallas kernels  4.3 us (30%)
  waiting for transfers between devices  3.72 us (26%)
  between operations  0.74 us (5%)
    ppermute x3, starting transfers between devices, turn(): lax.ppermute(x, 'sp', [(i, (i + by * cores) % peers) for i in range(peers)])  4.6 us
    pallas_call x9, Pallas kernels, call(): pl.pallas_call(body, out_shape=pltpu.HBM(outs.shape, outs.dtype) if away...  4.3 us
    ppermute x3, waiting for transfers between devices, turn(): lax.ppermute(x, 'sp', [(i, (i + by * cores) % peers) for i in range(peers)])  3.71 us
    ppermute x4, starting transfers between devices, swap(): lax.ppermute(x, 'sp', [(i, i // cores * cores + cores - 1 - i % cores) fo...  0.76 us
  transfers between devices with their start and end apart: 7, of which 2 were waited for; matrix products, arithmetic and copies ran while one was open for 0% of the time, Pallas kernels for 17%

profile of v6, /device:TPU:0, one launch (start us, length us, event | category | flops | bytes accessed | tf_op | source)
XLA Modules:
  0.0 14.2 jit_solution(18279427972232136204)
XLA Ops:
  0.0 1.0 %conditional.3 = ((bf16[512,128]{1,0:T(8,128)(2,1)S(1)}, bf16[528,128]{1,0:T(8,128)(2,1)S(1)})) conditional(s32[]{:T(128)} %convert_element_type.8, () %tuple.26, (bf16[1,128,4,128]{3,2,1,0:T(4,128)(2,1)}, bf16[1,128,4,128]{3,2,1,0:T(4,128)(2,1)}) %tuple.27), branch_computations={%region_0.1_spmd, %region_1.2_spmd} | conditional | bytes 8 | solution.py:333
  0.0 1.0 %branch_1_fun.3 = (bf16[512,128]{1,0:T(8,128)(2,1)S(1)}, bf16[528,128]{1,0:T(8,128)(2,1)S(1)}) custom-call(bf16[512,128]{1,0:T(8,128)(2,1)} %bitcast.13, bf16[512,128]{1,0:T(8,128)(2,1)} %bitcast.15), custom_call_target="tpu_custom_call" | custom-call | tf_op jit(solution)/shard_map/cond/branch_1_fun/pallas_call | solution.py:288
  1.0 0.0 copy-start
  1.0 2.0 %collective-permute-start.4 = (bf16[512,128]{1,0:T(8,128)(2,1)S(1)}, bf16[512,128]{1,0:T(8,128)(2,1)S(1)}, u32[]{:S(2)}, u32[]{:S(2)}) collective-permute-start(bf16[512,128]{1,0:T(8,128)(2,1)S(1)} %get-tuple-element.90), channel_id=1, source_target_pairs={{0,16},{8,24},{16,0},{24,8},{1,17},{9,25},{17,1},{25,9},{2,18},{10... | collective-permute-start | bytes 393224 | tf_op jit(solution)/shard_map/ppermute | solution.py:309
  3.0 0.0 collective-permute-start.2
  3.7 0.4 %collective-permute-start.5 = (bf16[528,128]{1,0:T(8,128)(2,1)S(1)}, bf16[528,128]{1,0:T(8,128)(2,1)S(1)}, u32[]{:S(2)}, u32[]{:S(2)}) collective-permute-start(bf16[528,128]{1,0:T(8,128)(2,1)S(1)} %get-tuple-element.96), channel_id=1, source_target_pairs={{0,16},{8,24},{16,0},{24,8},{1,17},{9,25},{17,1},{25,9},{2,18},{10... | collective-permute-start | bytes 405512 | tf_op jit(solution)/shard_map/ppermute | solution.py:309
  4.1 0.0 copy-done
  4.1 0.2 %collective-permute-start.3 = (bf16[1,128,4,128]{3,2,1,0:T(4,128)(2,1)S(1)}, bf16[1,128,4,128]{3,2,1,0:T(4,128)(2,1)S(1)}, u32[]{:S(2)}, u32[]{:S(2)}) collective-permute-start(bf16[1,128,4,128]{3,2,1,0:T(4,128)(2,1)S(1)} %copy-done), channel_id=1, source_target_pairs={{0,8},{8,0},{16,24},{24,16},{1,9},{9,1},{17,25},{25,17},{2,10},{10... | collective-permute-start | bytes 393224 | tf_op jit(solution)/shard_map/ppermute | solution.py:312
  4.4 2.8 %collective-permute-done.4.refs_1_ = bf16[512,128]{1,0:T(8,128)(2,1)S(1)} collective-permute-done((bf16[512,128]{1,0:T(8,128)(2,1)S(1)}, bf16[512,128]{1,0:T(8,128)(2,1)S(1)}, u32[]{:S(2)}, u32[]{:S(2)}) %collective-permute-start.4) | collective-permute-done | bytes 131104 | tf_op jit(solution)/shard_map/ppermute | solution.py:309
  7.1 0.0 collective-permute-start.6
  7.1 0.5 %collective-permute-start.1 = (f32[1,8,128]{2,1,0:T(8,128)S(1)}, f32[1,8,128]{2,1,0:T(8,128)S(1)}, u32[]{:S(2)}, u32[]{:S(2)}) collective-permute-start(f32[1,8,128]{2,1,0:T(8,128)S(1)} %get-tuple-element.84.refs_0_), channel_id=1, source_target_pairs={{0,8},{8,0},{16,24},{24,16},{1,9},{9,1},{17,25},{25,17},{2,10},{10... | collective-permute-start | bytes 12296 | tf_op jit(solution)/shard_map/ppermute | solution.py:312
  7.7 1.1 %shard_map.57 = (bf16[4,256,128]{2,1,0:T(8,128)(2,1)S(1)}, bf16[512,128]{1,0:T(8,128)(2,1)S(1)}, bf16[512,128]{1,0:T(8,128)(2,1)S(1)}, f32[8,128]{1,0:T(8,128)S(1)}) custom-call(bf16[512,128]{1,0:T(8,128)(2,1)} %bitcast.16, bf16[512,128]{1,0:T(8,128)(2,1)} %bitcast.12, bf16[512,128]{1,0:T(8,128)(2,1)} %bitcast.14, f32[1,128]{1,0:T(1,128)} %bitcast.19), custom_call_target="tpu_custom_call" | custom-call | tf_op jit(solution)/shard_map/pallas_call | solution.py:288
  8.8 0.0 collective-permute-done.1.refs_1_
  8.8 0.0 collective-permute-done.2
  8.8 0.6 %shard_map.59 = (bf16[2,4,256,128]{3,2,1,0:T(8,128)(2,1)S(1)}, f32[4,256,128]{2,1,0:T(8,128)S(1)}, f32[8,128]{1,0:T(8,128)S(1)}, f32[2,1,8,128]{3,2,1,0:T(8,128)S(1)}) custom-call(bf16[4,256,128]{2,1,0:T(8,128)(2,1)S(1)} %get-tuple-element.80.stacked, bf16[512,128]{1,0:T(8,128)(2,1)S(1)} %get-tuple-element.81.key_heads, ...), custom_call_target="tpu_custom_call" | custom-call | tf_op jit(solution)/shard_map/pallas_call | solution.py:288
  9.4 2.2 %collective-permute-start.7 = (f32[2,1,8,128]{3,2,1,0:T(8,128)S(1)}, f32[2,1,8,128]{3,2,1,0:T(8,128)S(1)}, u32[]{:S(2)}, u32[]{:S(2)}) collective-permute-start(f32[2,1,8,128]{3,2,1,0:T(8,128)S(1)} %get-tuple-element.88.pair), channel_id=1, source_target_pairs={{0,16},{8,24},{16,0},{24,8},{1,17},{9,25},{17,1},{25,9},{2,18},{10... | collective-permute-start | bytes 24584 | tf_op jit(solution)/shard_map/ppermute | solution.py:309
  11.7 0.0 collective-permute-done.3
  11.7 0.6 %shard_map.60 = (bf16[1,4,256,128]{3,2,1,0:T(8,128)(2,1)S(1)}, f32[4,256,128]{2,1,0:T(8,128)S(1)}, f32[4,256,128]{2,1,0:T(8,128)S(1)}, f32[8,128]{1,0:T(8,128)S(1)}, f32[2,1,8,128]{3,2,1,0:T(8,128)S(1)}) custom-call(bf16[4,256,128]{2,1,0:T(8,128)(2,1)S(1)} %get-tuple-element.80.stacked, bf16[2,4,256,128]{3,2,1,0:T(8,128)(2,1)S(1)} %get-tuple-element.85.near_raised, ...), custom_call_target="tpu_custom_call" | custom-call | tf_op jit(solution)/shard_map/pallas_call | solution.py:288
  12.3 0.0 collective-permute-done.5.refs_0_
  12.3 0.0 collective-permute-done.6.refs_1_
  12.4 0.9 %collective-permute-done.7.refs_0_ = f32[2,1,8,128]{3,2,1,0:T(8,128)S(1)} collective-permute-done((f32[2,1,8,128]{3,2,1,0:T(8,128)S(1)}, f32[2,1,8,128]{3,2,1,0:T(8,128)S(1)}, u32[]{:S(2)}, u32[]{:S(2)}) %collective-permute-start.7) | collective-permute-done | bytes 8224 | tf_op jit(solution)/shard_map/ppermute | solution.py:309
  13.3 0.9 %conditional.5 = (bf16[1,128,4,128]{3,2,1,0:T(4,128)(2,1)}) conditional(s32[]{:T(128)} %convert_element_type.7, (f32[4,256,128]{2,1,0:T(8,128)S(1)}, f32[8,128]{1,0:T(8,128)S(1)}, f32[2,1,8,128]{3,2,1,0:T(8,128)S(1)}, f32[2,1,8,128]{3,2,1,0:T(8,128)S(1)}) %tuple.31, bf16[512,128]{1,0:T(8,128)(2,1)} %get-tuple-element.109), branch_computations={%region_4.5_spmd, %region_5.6_spmd} | conditional | bytes 8 | solution.py:404
  13.3 0.8 %branch_0_fun.5 = bf16[512,128]{1,0:T(8,128)(2,1)} custom-call(f32[4,256,128]{2,1,0:T(8,128)S(1)} %get-tuple-element.55.summed, f32[8,128]{1,0:T(8,128)S(1)} %get-tuple-element.56.gain, f32[2,1,8,128]{3,2,1,0:T(8,128)S(1)} %get-tuple-element.57.near_pair, f32[2,1,8,128]{3,2,1,0:T(8,128)S(1)} %get-tuple-element.58.refs_0_), custom_call_target="tpu_custom_call" | custom-call | tf_op jit(solution)/shard_map/cond/branch_0_fun/pallas_call | solution.py:288
  (5 shorter events, 0.1 us)
Async XLA Ops:
  1.0 3.1 %copy-start = (bf16[1,128,4,128]{3,2,1,0:T(4,128)(2,1)S(1)}, bf16[1,128,4,128]{3,2,1,0:T(4,128)(2,1)}, u32[]{:S(2)}) copy-start(bf16[1,128,4,128]{3,2,1,0:T(4,128)(2,1)} %param.13) | copy-start | bytes 393220
  1.0 6.1 %collective-permute-start.4 = (bf16[512,128]{1,0:T(8,128)(2,1)S(1)}, bf16[512,128]{1,0:T(8,128)(2,1)S(1)}, u32[]{:S(2)}, u32[]{:S(2)}) collective-permute-start(bf16[512,128]{1,0:T(8,128)(2,1)S(1)} %get-tuple-element.90), channel_id=1, source_target_pairs={{0,16},{8,24},{16,0},{24,8},{1,17},{9,25},{17,1},{25,9},{2,18},{10... | collective-permute-start | bytes 393224 | tf_op jit(solution)/shard_map/ppermute | solution.py:309
  3.0 5.8 %collective-permute-start.2 = (bf16[1,128,4,128]{3,2,1,0:T(4,128)(2,1)}, bf16[1,128,4,128]{3,2,1,0:T(4,128)(2,1)S(1)}, u32[]{:S(2)}, u32[]{:S(2)}) collective-permute-start(bf16[1,128,4,128]{3,2,1,0:T(4,128)(2,1)} %param.12), channel_id=1, source_target_pairs={{0,8},{8,0},{16,24},{24,16},{1,9},{9,1},{17,25},{25,17},{2,10},{10... | collective-permute-start | bytes 393224 | tf_op jit(solution)/shard_map/ppermute | solution.py:312
  3.7 8.6 %collective-permute-start.5 = (bf16[528,128]{1,0:T(8,128)(2,1)S(1)}, bf16[528,128]{1,0:T(8,128)(2,1)S(1)}, u32[]{:S(2)}, u32[]{:S(2)}) collective-permute-start(bf16[528,128]{1,0:T(8,128)(2,1)S(1)} %get-tuple-element.96), channel_id=1, source_target_pairs={{0,16},{8,24},{16,0},{24,8},{1,17},{9,25},{17,1},{25,9},{2,18},{10... | collective-permute-start | bytes 405512 | tf_op jit(solution)/shard_map/ppermute | solution.py:309
  4.1 7.6 %collective-permute-start.3 = (bf16[1,128,4,128]{3,2,1,0:T(4,128)(2,1)S(1)}, bf16[1,128,4,128]{3,2,1,0:T(4,128)(2,1)S(1)}, u32[]{:S(2)}, u32[]{:S(2)}) collective-permute-start(bf16[1,128,4,128]{3,2,1,0:T(4,128)(2,1)S(1)} %copy-done), channel_id=1, source_target_pairs={{0,8},{8,0},{16,24},{24,16},{1,9},{9,1},{17,25},{25,17},{2,10},{10... | collective-permute-start | bytes 393224 | tf_op jit(solution)/shard_map/ppermute | solution.py:312
  7.1 5.2 %collective-permute-start.6 = (bf16[512,128]{1,0:T(8,128)(2,1)S(1)}, bf16[512,128]{1,0:T(8,128)(2,1)S(1)}, u32[]{:S(2)}, u32[]{:S(2)}) collective-permute-start(bf16[512,128]{1,0:T(8,128)(2,1)S(1)} %collective-permute-done.4.refs_1_), channel_id=1, source_target_pairs={{0,8},{8,0},{16,24},{24,16},{1,9},{9,1},{17,25},{25,17},{2,10},{10... | collective-permute-start | bytes 393224 | tf_op jit(solution)/shard_map/ppermute | solution.py:312
  7.1 1.7 %collective-permute-start.1 = (f32[1,8,128]{2,1,0:T(8,128)S(1)}, f32[1,8,128]{2,1,0:T(8,128)S(1)}, u32[]{:S(2)}, u32[]{:S(2)}) collective-permute-start(f32[1,8,128]{2,1,0:T(8,128)S(1)} %get-tuple-element.84.refs_0_), channel_id=1, source_target_pairs={{0,8},{8,0},{16,24},{24,16},{1,9},{9,1},{17,25},{25,17},{2,10},{10... | collective-permute-start | bytes 12296 | tf_op jit(solution)/shard_map/ppermute | solution.py:312
  9.4 3.9 %collective-permute-start.7 = (f32[2,1,8,128]{3,2,1,0:T(8,128)S(1)}, f32[2,1,8,128]{3,2,1,0:T(8,128)S(1)}, u32[]{:S(2)}, u32[]{:S(2)}) collective-permute-start(f32[2,1,8,128]{3,2,1,0:T(8,128)S(1)} %get-tuple-element.88.pair), channel_id=1, source_target_pairs={{0,16},{8,24},{16,0},{24,8},{1,17},{9,25},{17,1},{25,9},{2,18},{10... | collective-permute-start | bytes 24584 | tf_op jit(solution)/shard_map/ppermute | solution.py:309
